TPU v7x, 128 devices: a whole 4x4x4 slice. The times are simulated.
128 devices in a mesh: kv: 16 (over z, y), tp: 8 (over x, core).
Axes of the slice: x: 4, y: 4, z: 4, core: 2. Of those that a mesh axis runs over, the one named last changes fastest.
Arguments:
- tokens: bfloat16 [64, 4096], P(None, 'kv'), may hold values from -170 to 170
- mix_gain: float32 [4096], P('kv'), may hold values from 0.1 to 1.9
- w_query: bfloat16 [4096, 2048], P('kv', 'tp'), may hold values from -0.09375 to 0.09375
- w_key: bfloat16 [4096, 512], P('kv', 'tp'), may hold values from -0.09375 to 0.09375
- w_value: bfloat16 [4096, 512], P('kv', 'tp'), may hold values from -0.09375 to 0.09375
- w_forget: bfloat16 [4096, 32], P('kv', 'tp'), may hold values from -0.09375 to 0.09375
- query_gain: float32 [64], replicated, may hold values from 0.1 to 1.9
- key_cache: bfloat16 [64, 8, 64, 16384], P(None, 'tp', None, 'kv'), may hold values from -1300 to 1300
- value_cache: bfloat16 [64, 8, 64, 16384], P(None, 'tp', None, 'kv'), may hold values from -8 to 8
- decay_cache: float32 [64, 32, 16384], P(None, 'tp', 'kv'), may hold values from -2131.92 to 0, as said below
- w_out: bfloat16 [2048, 4096], P('tp', 'kv'), may hold values from -1 to 1
- mlp_gain: float32 [4096], P('kv'), may hold values from 0.1 to 1.9
- w_up: bfloat16 [4096, 16384], P('kv', 'tp'), may hold values from -0.09375 to 0.09375
- w_down: bfloat16 [16384, 4096], P('tp', 'kv'), may hold values from -0.046875 to 0.046875
Outputs:
- layer_out: bfloat16 [64, 4096], P(None, 'kv')
Inputs may be any that keep to these rules, and one draw needn't show every extreme that they name: `decay_cache`: each entry is the sum of the non-positive log forget gates of the later cached positions of its sequence and head: 0 at the last cached position, never smaller at a later position.
All inputs are finite; a program needn't handle non-finite values.
Results may differ from a plain program's by a relative error of at most 0.015.
Values may be sent and summed in bfloat16 or wider, within the bound.
No kernel may reach another device: no remote copies, remote signals or barrier semaphores. Data moves between devices by JAX's collectives and lax.ppermute only.
A program may use at most 64 MiB of HBM per device.

v0:
```python
import jax
import jax.numpy as jnp
from jax import lax
from jax.sharding import Mesh
from jax.sharding import PartitionSpec as P

D = 4096
HEAD_DIM = 64
KV = ("kv_0", "kv_1")


EPS = 1e-06


def sent_to_all(array, axis):
    copies = jnp.broadcast_to(array, (lax.axis_size(axis), *array.shape))
    return lax.all_to_all(copies, axis, split_axis=0, concat_axis=0, tiled=True)


def over_copies(array, axis):
    return sent_to_all(array, axis).sum(axis=0)


def in_one(arrays, axis):
    ends = [0]
    for a in arrays:
        ends.append(ends[-1] + a.size)
    subtotal = over_copies(jnp.concatenate([a.ravel() for a in arrays]), axis)
    return tuple((subtotal[b:e].reshape(a.shape) for a, b, e in zip(arrays, ends, ends[1:])))


def gathered_once(array, axis):
    leaves = jax.tree.leaves(array)
    sequence = sorted(range(len(leaves)), key=lambda k: -leaves[k].size)
    width = (1, *leaves[sequence[0]].shape)[-1]
    lines = [
        jnp.pad(leaves[k].reshape(-1), (0, -leaves[k].size % width)).reshape(-1, width)
        for k in sequence
    ]
    both, at, found = (lax.all_gather(jnp.concatenate(lines), axis), 0, {})
    for k, line in zip(sequence, lines):
        piece = both[:, at : at + len(line)].reshape(len(both), -1)
        found[k] = piece[:, : leaves[k].size].reshape(-1, *leaves[k].shape)
        at += len(line)
    numbers = iter(range(len(leaves)))
    return jax.tree.map(lambda _: found[next(numbers)], array)


def merged_by_axis(array, axes, combine):
    for axis in axes:
        pieces = gathered_once(array, axis)
        array = jax.tree.map(lambda part: part[0], pieces)
        for k in range(1, lax.axis_size(axis)):
            array = combine(array, jax.tree.map(lambda part: part[k], pieces))
    return array


def over_copies_2(array, axis):
    return sent_to_all(array, axis).astype(jnp.float32).sum(axis=0)


def cut_along(array, dim, length):
    before, after = (array.shape[:dim], array.shape[dim + 1 :])
    return jnp.moveaxis(array.reshape(*before, length, -1, *after), dim, 0)


def sum_at_owner(array, axis, dim):
    length = lax.axis_size(axis)
    pieces = lax.all_to_all(cut_along(array, dim, length), axis, 0, 0, tiled=True)
    return jnp.sum(pieces, axis=0)


def joined_along(pieces, dim):
    shape = list(pieces.shape[1:])
    shape[dim] *= pieces.shape[0]
    return jnp.moveaxis(pieces, 0, dim).reshape(shape)


def collect(array, axis, dim):
    pieces = sent_to_all(array, axis)
    return joined_along(pieces, dim)


def merge_parts(left_part, right_part):
    peak_score = jnp.maximum(left_part[0], right_part[0])
    left_factor = jnp.exp(left_part[0] - peak_score)
    right_factor = jnp.exp(right_part[0] - peak_score)
    return (
        peak_score,
        left_part[1] * left_factor + right_part[1] * right_factor,
        left_part[2] * left_factor[..., None] + right_part[2] * right_factor[..., None],
    )


def shards(
    tokens,
    mix_gain,
    w_query,
    w_key,
    w_value,
    w_forget,
    query_gain,
    key_cache,
    value_cache,
    decay_cache,
    w_out,
    mlp_gain,
    w_up,
    w_down,
):
    row_count = tokens.shape[0]
    local_heads = w_forget.shape[1]
    local_groups = key_cache.shape[1]
    sharing = local_heads // local_groups
    score_scale = HEAD_DIM ** (-0.5)
    stream = tokens.astype(jnp.float32)
    squares_mix = jnp.sum(stream * stream, axis=1)
    normed_mix = (stream * mix_gain).astype(jnp.bfloat16)
    query_terms = jnp.dot(normed_mix, w_query, preferred_element_type=jnp.float32)
    key_terms = jnp.dot(normed_mix, w_key, preferred_element_type=jnp.float32)
    value_terms = jnp.dot(normed_mix, w_value, preferred_element_type=jnp.float32)
    forget_terms = jnp.dot(normed_mix, w_forget, preferred_element_type=jnp.float32)
    query_raw, key_raw, value_raw, forget_raw, total_mix = in_one(
        (query_terms, key_terms, value_terms, forget_terms, squares_mix), KV
    )
    scale_mix = lax.rsqrt(total_mix / D + EPS)[:, None]
    heads_raw = (scale_mix * query_raw).reshape(row_count, local_heads, HEAD_DIM)
    inverse = lax.rsqrt(jnp.mean(heads_raw * heads_raw, axis=-1, keepdims=True) + EPS)
    query = (heads_raw * inverse * query_gain).astype(jnp.bfloat16)
    query = query.reshape(row_count, local_groups, sharing, HEAD_DIM)
    key_new = (scale_mix * key_raw).reshape(row_count, local_groups, HEAD_DIM).astype(jnp.bfloat16)
    value_new = (
        (scale_mix * value_raw).reshape(row_count, local_groups, HEAD_DIM).astype(jnp.bfloat16)
    )
    log_forget = jax.nn.log_sigmoid(scale_mix * forget_raw).reshape(
        row_count, local_groups, sharing
    )
    decay = decay_cache.reshape(row_count, local_groups, sharing, -1)
    scores = (
        jnp.einsum("bgjd,bgdp->bgjp", query, key_cache, preferred_element_type=jnp.float32)
        * score_scale
    )
    scores = scores + decay + log_forget[..., None]
    own_score = (
        jnp.einsum("bgjd,bgd->bgj", query, key_new, preferred_element_type=jnp.float32)
        * score_scale
    )
    local_peak = jnp.max(scores, axis=-1)
    weights = jnp.exp(scores - local_peak[..., None])
    summed = jnp.einsum(
        "bgjp,bgdp->bgjd",
        weights.astype(jnp.bfloat16),
        value_cache,
        preferred_element_type=jnp.float32,
    )
    far_peak, mass_sum, summed = merged_by_axis(
        (local_peak, jnp.sum(weights, axis=-1), summed), KV, merge_parts
    )
    peak_score = jnp.maximum(far_peak, own_score)
    keep = jnp.exp(far_peak - peak_score)
    mass_sum = mass_sum * keep
    summed = summed * keep[..., None]
    own_weight = jnp.exp(own_score - peak_score)
    totals = mass_sum + own_weight
    own_rounded = lax.optimization_barrier(own_weight.astype(jnp.bfloat16)).astype(jnp.float32)
    summed = summed + own_rounded[..., None] * value_new.astype(jnp.float32)[:, :, None, :]
    head_output = summed / totals[..., None]
    attended = head_output.reshape(row_count, local_heads * HEAD_DIM).astype(jnp.bfloat16)
    attn_terms = jnp.dot(attended, w_out, preferred_element_type=jnp.float32)
    attn_out = over_copies_2(attn_terms.astype(jnp.bfloat16), "tp").astype(jnp.float32)
    attn_rounded = lax.optimization_barrier(attn_out.astype(jnp.bfloat16)).astype(jnp.float32)
    residual = (stream + attn_rounded).astype(jnp.bfloat16)
    residual_wide = residual.astype(jnp.float32)
    squares_mlp = jnp.sum(residual_wide * residual_wide, axis=1)
    normed_mlp = (residual_wide * mlp_gain).astype(jnp.bfloat16)
    up_terms = jnp.dot(normed_mlp, w_up, preferred_element_type=jnp.float32)
    square_columns = jnp.broadcast_to(squares_mlp[:, None], (row_count, lax.axis_size(KV)))
    up_share, total_columns = (sum_at_owner(up_terms, KV, 1), sum_at_owner(square_columns, KV, 1))
    scale_mlp = lax.rsqrt(total_columns[:, 0] / D + EPS)[:, None]
    hidden_share = jnp.square(jax.nn.relu(scale_mlp * up_share)).astype(jnp.bfloat16)
    down_terms = jnp.dot(collect(hidden_share, KV, 1), w_down, preferred_element_type=jnp.float32)
    mlp_out = over_copies_2(down_terms.astype(jnp.bfloat16), "tp").astype(jnp.float32)
    mlp_rounded = lax.optimization_barrier(mlp_out.astype(jnp.bfloat16)).astype(jnp.float32)
    return (residual_wide + mlp_rounded).astype(jnp.bfloat16)


def solution(mesh):
    split = Mesh(mesh.devices.reshape(4, 4, mesh.shape["tp"]), ("kv_0", "kv_1", "tp"))
    return jax.shard_map(
        shards,
        mesh=split,
        in_specs=(
            P(None, KV),
            P(KV),
            P(KV, "tp"),
            P(KV, "tp"),
            P(KV, "tp"),
            P(KV, "tp"),
            P(),
            P(None, "tp", None, KV),
            P(None, "tp", None, KV),
            P(None, "tp", KV),
            P("tp", KV),
            P(KV),
            P(KV, "tp"),
            P("tp", KV),
        ),
        out_specs=P(None, KV),
        check_vma=False,
    )
```

profile of v0, /device:TPU:1, one launch (start us, length us, event | category | flops | bytes accessed | tf_op | source)
XLA Modules:
  0.0 144.4 jit_solution(328288625187221567)
XLA Ops:
  0.0 1.0 fusion.20
  1.0 0.9 fusion.45
  2.0 0.9 fusion.43
  3.0 0.9 fusion.41
  4.0 1.1 convolution_bitcast_fusion.1
  5.2 0.8 broadcast_in_dim.8
  6.0 30.8 %all_to_all.31 = f32[16,1,24896]{2,1,0:T(1,128)S(1)} all-to-all(f32[16,1,24896]{2,1,0:T(1,128)S(1)} %broadcast_in_dim.8), channel_id=1, replica_groups=mesh['kv_0'=4,'kv_1'=4,'tp'=8] {'kv_0','kv_1'}, dimensions={0} | all-to-all | bytes 3186688 | tf_op jit(solution)/shard_map/all_to_all | solution.py:17
  36.8 1.0 reduce_sum.88
  38.4 0.9 multiply_convert_fusion
  39.3 4.9 %fusion.71 = (f32[64,4]{1,0:T(8,128)S(1)}, f32[64,4,1024]{2,1,0:T(4,128)S(1)}) fusion(f32[64,4]{1,0:T(8,128)S(1)} %fusion.37, f32[64,4,1024]{2,1,0:T(4,128)} %param.23, bf16[64,4,64]{2,1,0:T(4,128)(2,1)S(1)} %multiply_convert_fusion, bf16[64,1,64,1024]{3,2,1,0:T(8,128)(2,1)} %param.21), kind=kOutput, calls=%fused_computation.120 | convolution fusion | flops 34602752 | bytes 10520576 | tf_op jit(solution)/shard_map/bgjd,bgdp->bgjp/dot_general | solution.py:140
  44.4 0.5 fusion.13
  44.9 5.7 %fusion = f32[64,4,64]{2,1,0:T(4,128)S(1)} fusion(bf16[64,1,64,1024]{3,2,1,0:T(8,128)(2,1)} %param.22, f32[64,4,1024]{2,1,0:T(4,128)S(1)} %get-tuple-element.49, f32[64,4]{1,0:T(8,128)S(1)} %get-tuple-element.48), kind=kOutput, calls=%fused_computation | convolution fusion | flops 34078720 | bytes 9503744 | tf_op jit(solution)/shard_map/bgjp,bgdp->bgjd/dot_general | solution.py:150
  51.0 10.3 %all-gather.2 = f32[4,264,64]{1,2,0:T(8,128)S(1)} all-gather(f32[1,264,64]{1,2,0:T(8,128)S(1)} %maximum_bitcast_fusion), channel_id=2, replica_groups=mesh['kv_0'=4,'kv_1'=4,'tp'=8] {'kv_0'}, dimensions={0}, use_global_device_ids=true | all-gather | bytes 337920 | tf_op jit(solution)/shard_map/all_gather | solution.py:40
  62.8 10.1 %all-gather.3 = f32[4,264,64]{1,2,0:T(8,128)S(1)} all-gather(f32[1,264,64]{1,2,0:T(8,128)S(1)} %maximum_bitcast_fusion.1), channel_id=3, replica_groups=mesh['kv_0'=4,'kv_1'=4,'tp'=8] {'kv_1'}, dimensions={0}, use_global_device_ids=true | all-gather | bytes 337920 | tf_op jit(solution)/shard_map/all_gather | solution.py:40
  78.4 17.5 %all_to_all.32 = bf16[8,64,256]{2,1,0:T(8,128)(2,1)S(1)} all-to-all(bf16[8,64,256]{2,1,0:T(8,128)(2,1)S(1)} %broadcast_in_dim.9), channel_id=1, replica_groups=mesh['kv_0'=4,'kv_1'=4,'tp'=8] {'tp'}, dimensions={0} | all-to-all | bytes 524288 | tf_op jit(solution)/shard_map/all_to_all | solution.py:17
  96.1 0.6 transpose.34
  96.7 3.5 %all-to-all-start.2 = ((f32[16,64,1]{1,2,0:T(1,128)}), f32[16,64,1]{1,2,0:T(1,128)S(1)}, u32[]{:S(2)}, u32[]{:S(2)}) async-start(f32[16,64,1]{1,2,0:T(1,128)} %transpose.34), calls=%async_computation.2 | async-start | bytes 16384 | tf_op jit(solution)/shard_map/all_to_all | solution.py:69
  100.5 0.8 copy.190
  101.4 5.2 %all-to-all-done.2 = f32[16,64,1]{1,2,0:T(1,128)S(1)} async-done(((f32[16,64,1]{1,2,0:T(1,128)}), f32[16,64,1]{1,2,0:T(1,128)S(1)}, u32[]{:S(2)}, u32[]{:S(2)}) %all-to-all-start.2) | async-done | bytes 4128 | tf_op jit(solution)/shard_map/all_to_all | solution.py:69
  106.5 3.6 %all-to-all-start.3 = ((f32[16,64,128]{2,1,0:T(8,128)}), f32[16,64,128]{2,1,0:T(8,128)S(1)}, u32[]{:S(2)}, u32[]{:S(2)}) async-start(f32[16,64,128]{2,1,0:T(8,128)} %bitcast.165), calls=%async_computation.3 | async-start | bytes 1048576 | tf_op jit(solution)/shard_map/all_to_all | solution.py:69
  110.2 9.2 %all-to-all-done.3 = f32[16,64,128]{2,1,0:T(8,128)S(1)} async-done(((f32[16,64,128]{2,1,0:T(8,128)}), f32[16,64,128]{2,1,0:T(8,128)S(1)}, u32[]{:S(2)}, u32[]{:S(2)}) %all-to-all-start.3) | async-done | bytes 524320 | tf_op jit(solution)/shard_map/all_to_all | solution.py:69
  119.6 10.1 %all_to_all.33 = bf16[16,64,128]{2,1,0:T(8,128)(2,1)S(1)} all-to-all(bf16[16,64,128]{2,1,0:T(8,128)(2,1)S(1)} %broadcast_in_dim.10), channel_id=1, replica_groups=mesh['kv_0'=4,'kv_1'=4,'tp'=8] {'kv_0','kv_1'}, dimensions={0} | all-to-all | bytes 524288 | tf_op jit(solution)/shard_map/all_to_all | solution.py:17
  130.1 13.7 %all_to_all.34 = bf16[8,64,256]{2,1,0:T(8,128)(2,1)S(1)} all-to-all(bf16[8,64,256]{2,1,0:T(8,128)(2,1)S(1)} %broadcast_in_dim.11), channel_id=1, replica_groups=mesh['kv_0'=4,'kv_1'=4,'tp'=8] {'tp'}, dimensions={0} | all-to-all | bytes 524288 | tf_op jit(solution)/shard_map/all_to_all | solution.py:17
  143.8 0.6 fusion.24
  (118 shorter events, 9.1 us)
Async XLA Ops:
  0.0 100.2 %copy-start = (bf16[256,2048]{1,0:T(8,128)(2,1)S(1)}, bf16[256,2048]{1,0:T(8,128)(2,1)}, u32[]{:S(2)}) copy-start(bf16[256,2048]{1,0:T(8,128)(2,1)} %param.26) | copy-start | bytes 3145732
  44.9 33.3 %copy-start.3 = (bf16[256,256]{1,0:T(8,128)(2,1)S(1)}, bf16[256,256]{1,0:T(8,128)(2,1)}, u32[]{:S(2)}) copy-start(bf16[256,256]{1,0:T(8,128)(2,1)} %param.24) | copy-start | bytes 393220
  50.6 45.3 %copy-start.1 = (bf16[64,256]{1,0:T(8,128)(2,1)S(1)}, bf16[64,256]{1,0:T(8,128)(2,1)}, u32[]{:S(2)}) copy-start(bf16[64,256]{1,0:T(8,128)(2,1)} %param.14) | copy-start | bytes 98308
  50.6 49.6 %copy-start.4 = (f32[256]{0:T(256)S(1)}, f32[256]{0:T(256)}, u32[]{:S(2)}) copy-start(f32[256]{0:T(256)} %param.25) | copy-start | bytes 3076
  61.4 68.3 %copy-start.2 = (bf16[2048,256]{1,0:T(8,128)(2,1)S(1)}, bf16[2048,256]{1,0:T(8,128)(2,1)}, u32[]{:S(2)}) copy-start(bf16[2048,256]{1,0:T(8,128)(2,1)} %param.27) | copy-start | bytes 3145732
  96.7 9.8 %all-to-all-start.2 = ((f32[16,64,1]{1,2,0:T(1,128)}), f32[16,64,1]{1,2,0:T(1,128)S(1)}, u32[]{:S(2)}, u32[]{:S(2)}) async-start(f32[16,64,1]{1,2,0:T(1,128)} %transpose.34), calls=%async_computation.2 | async-start | bytes 16384 | tf_op jit(solution)/shard_map/all_to_all | solution.py:69
  106.5 12.9 %all-to-all-start.3 = ((f32[16,64,128]{2,1,0:T(8,128)}), f32[16,64,128]{2,1,0:T(8,128)S(1)}, u32[]{:S(2)}, u32[]{:S(2)}) async-start(f32[16,64,128]{2,1,0:T(8,128)} %bitcast.165), calls=%async_computation.3 | async-start | bytes 1048576 | tf_op jit(solution)/shard_map/all_to_all | solution.py:69
where the time goes:
time: 145 us; the launch traced here: 144 us
  blocking collectives  92.5 us (64%)
  matrix products  15.5 us (11%)
  waiting for transfers between devices  14.4 us (10%)
  local copies, waits for them, and re-layouts  9.15 us (6%)
  starting transfers between devices  7.05 us (5%)
  other arithmetic  5.22 us (4%)
    all_to_all x4, blocking collectives, sent_to_all(): return lax.all_to_all(copies, axis, split_axis=0, concat_axis=0, tiled=True)  72.1 us
    all_gather x2, blocking collectives, gathered_once(): both, at, found = (lax.all_gather(jnp.concatenate(lines), axis), 0, {})  20.5 us
    all_to_all x2, waiting for transfers between devices, sum_at_owner(): lax.all_to_all(cut_along(array, dim, length), axis, 0, 0, tiled=True)  14.4 us
    all_to_all x2, starting transfers between devices, sum_at_owner(): lax.all_to_all(cut_along(array, dim, length), axis, 0, 0, tiled=True)  7.05 us
    dot_general x1, matrix products, shards(): jnp.einsum('bgjp,bgdp->bgjd', weights.astype(jnp.bfloat16), value_cache,...  5.74 us
    dot_general x1, matrix products, shards(): jnp.einsum('bgjd,bgdp->bgjp', query, key_cache, preferred_element_type=jn...  4.89 us
  transfers between devices with their start and end apart: 2, of which 2 were waited for; matrix products, arithmetic and copies ran while one was open for 1% of the time, Pallas kernels for 0%

commit v1 on v0

v1 whole, which is shorter than its diff:
```python
import functools

import jax
import jax.numpy as jnp
from jax import lax
from jax.experimental import pallas as pl
from jax.experimental.pallas import tpu as pltpu
from jax.sharding import PartitionSpec as P

D = 4096
HEAD_DIM = 64
EPS = 1e-06
BF = jnp.bfloat16
F32 = jnp.float32

VM = pl.BlockSpec(memory_space=pltpu.VMEM)
ANY = pl.BlockSpec(memory_space=pl.ANY)


def iota(shape, dim):
    return lax.broadcasted_iota(jnp.int32, shape, dim)


def dot(a, b):
    return jnp.dot(a, b, preferred_element_type=F32)


def dot_t(a, b):
    return lax.dot_general(a, b, (((1,), (1,)), ((), ())), preferred_element_type=F32)


def high(a):
    return a.astype(BF).astype(F32)


def column_to_row(column, width, at):
    n = column.shape[0]
    place = iota((n, width), 1) == iota((n, width), 0) + at
    return jnp.sum(jnp.where(place, column, 0.0), axis=0, keepdims=True)


def row_to_column(row, n, at):
    width = row.shape[1]
    place = iota((n, width), 1) == iota((n, width), 0) + at
    return jnp.sum(jnp.where(place, row, 0.0), axis=1, keepdims=True)


def call(kernel, outs, name, scratch=(), in_specs=None, limit=16 << 20):
    def run(*args):
        return pl.pallas_call(
            kernel,
            out_shape=outs,
            in_specs=in_specs or [VM] * len(args),
            out_specs=jax.tree.map(lambda _: VM, outs),
            scratch_shapes=list(scratch),
            compiler_params=pltpu.CompilerParams(vmem_limit_bytes=limit),
            name=name,
        )(*args)

    return run


def project_kernel(tokens, gain, w_query, w_key, w_value, w_forget, out):
    stream = tokens[...].astype(F32)
    squares = jnp.sum(stream * stream, axis=1, keepdims=True)
    normed = (stream * gain[...]).astype(BF)
    query = dot(normed, w_query[...]).astype(BF)
    key_value = dot_t(normed, jnp.concatenate([w_key[...], w_value[...]], axis=0))
    forget_w = w_forget[...].astype(F32)
    forget_w = jnp.concatenate([forget_w, forget_w, jnp.zeros((120, 256), F32)], axis=0)
    forget = dot_t(normed, forget_w.astype(BF))
    forget = jnp.where(iota(forget.shape, 1) < 4, high(forget), forget - high(forget))
    squares_high = high(squares)
    row_high = column_to_row(squares_high, 128, 64)
    row_low = column_to_row(squares - squares_high, 128, 64)
    line = iota((8, 128), 0)
    square_tile = jnp.where(line == 0, row_high, jnp.where(line == 1, row_low, 0.0))
    for p in range(16):
        t = p // 2
        out[p, 0:64, :] = query
        out[p, 64:72, 0:128] = key_value[8 * t : 8 * t + 8].astype(BF)
        out[p, 64:72, 128:256] = (forget[8 * t : 8 * t + 8] + square_tile).astype(BF)


def attend_kernel(
    parts, query_gain, key_hbm, value_hbm, decay_hbm, out,
    keys, values, decay, key_sem, value_sem, decay_sem, scales, query_rows, left, peaks, masses, sums,
):
    copies = []
    for g in range(8):
        rows = pl.ds(512 * g, 512)
        k_copy = pltpu.make_async_copy(key_hbm.at[rows], keys.at[g], key_sem.at[g])
        d_copy = pltpu.make_async_copy(decay_hbm.at[pl.ds(8 * g, 8)], decay.at[g], decay_sem.at[g])
        v_copy = pltpu.make_async_copy(value_hbm.at[rows], values.at[g], value_sem.at[g])
        k_copy.start()
        d_copy.start()
        v_copy.start()
        copies.append((k_copy, d_copy, v_copy))

    raw = parts[0, 0:64, :].astype(F32)
    extra = parts[0, 64:72, :].astype(F32)
    for i in range(1, 16):
        raw = raw + parts[i, 0:64, :].astype(F32)
        extra = extra + parts[i, 64:72, :].astype(F32)
    squares = row_to_column(extra[0:1, 128:256] + extra[1:2, 128:256], 64, 64)
    scale = lax.rsqrt(squares / D + EPS)
    scales[...] = jnp.broadcast_to(scale, (64, 128))
    heads = scale * raw
    head_of = iota((64, 256), 1) // HEAD_DIM
    power = heads * heads
    inverse = jnp.zeros((64, 256), F32)
    for h in range(4):
        mean = jnp.sum(jnp.where(head_of == h, power, 0.0), axis=1, keepdims=True) / HEAD_DIM
        inverse = jnp.where(head_of == h, lax.rsqrt(mean + EPS), inverse)
    gain = query_gain[...]
    gain = jnp.concatenate([gain, gain, gain, gain], axis=1)
    query = (heads * inverse * gain).astype(BF)

    repeat = (iota((256, 64), 0) // 4 == iota((256, 64), 1)).astype(BF)
    spread = dot(repeat, query)
    own_lanes = iota((256, 256), 1) // HEAD_DIM == iota((256, 256), 0) % 4
    spread = jnp.where(own_lanes, spread, 0.0)
    folded = spread[:, 0:128] + spread[:, 128:256]
    folded = folded + pltpu.roll(folded, 64, 1)
    query_rows[...] = folded
    wide = jnp.concatenate([folded] * 4, axis=1)
    block = iota((256, 512), 1) // HEAD_DIM == (iota((256, 512), 0) // 4) % 8
    left[...] = jnp.where(block, wide, 0.0).astype(BF)

    diagonal = iota((32, 512), 1) // HEAD_DIM == iota((32, 512), 0) // 4
    for g in range(8):
        k_copy, d_copy, v_copy = copies[g]
        rows = slice(32 * g, 32 * g + 32)
        k_copy.wait()
        scores = dot(left[rows, :], keys[g]) * (HEAD_DIM ** (-0.5))
        d_copy.wait()
        scores = scores + decay[g].reshape(32, 1024)
        peak = jnp.max(scores, axis=1, keepdims=True)
        weights = jnp.exp(scores - peak)
        mass = jnp.sum(weights, axis=1, keepdims=True)
        v_copy.wait()
        summed = dot_t(weights.astype(BF), values[g])
        summed = jnp.where(diagonal, summed, 0.0)
        summed = (summed[:, 0:128] + summed[:, 128:256]) + (summed[:, 256:384] + summed[:, 384:512])
        sums[rows, :] = summed + pltpu.roll(summed, 64, 1)
        peaks[rows, :] = jnp.broadcast_to(peak, (32, 128))
        masses[rows, :] = jnp.broadcast_to(mass, (32, 128))

    me = lax.axis_index("kv")
    tile = me // 2
    own_scale = scales[pl.ds(pl.multiple_of(8 * tile, 8), 8), :]
    key_value = (own_scale * extra[:, 0:128]).astype(BF)
    forget = extra[:, 128:256]
    forget = own_scale * (forget + pltpu.roll(forget, 124, 1))
    log_forget = -(jnp.maximum(-forget, 0.0) + jnp.log1p(jnp.exp(-jnp.abs(forget))))
    log_forget = jnp.where(iota((8, 128), 1) < 4, log_forget, 0.0)
    repeat8 = iota((32, 8), 0) // 4 == iota((32, 8), 1)
    key_value = dot(repeat8.astype(BF), key_value)
    log_forget = jnp.dot(
        repeat8.astype(F32), log_forget, preferred_element_type=F32, precision=lax.Precision.HIGHEST
    )
    mine = iota((32, 128), 1) == iota((32, 128), 0) % 4
    log_forget = jnp.sum(jnp.where(mine, log_forget, 0.0), axis=1, keepdims=True)
    at = pl.ds(pl.multiple_of(32 * tile, 32), 32)
    lower = iota((32, 128), 1) < 64
    own = jnp.sum(jnp.where(lower, query_rows[at, :] * key_value, 0.0), axis=1, keepdims=True)
    own = own * (HEAD_DIM ** (-0.5)) - log_forget
    value = jnp.where(lower, pltpu.roll(key_value, 64, 1), key_value)
    peak = peaks[at, :]
    own = jnp.where(me % 2 == 0, jnp.broadcast_to(own, (32, 128)), peak - 1e30)
    top = jnp.maximum(peak, own)
    keep = jnp.exp(peak - top)
    weight = jnp.exp(own - top)
    peaks[at, :] = top
    masses[at, :] = masses[at, :] * keep + weight
    sums[at, :] = sums[at, :] * keep + high(weight) * value

    mass = masses[...]
    level = peaks[...] + jnp.log(mass)
    result = sums[...] / mass
    first = iota((128, 128), 1) < 64
    out[0:128, :] = jnp.where(first, result[0:128], result[128:256]).astype(BF)
    place = iota((128, 128), 0) == iota((128, 128), 1)
    line = iota((8, 128), 0)
    packed = jnp.zeros((8, 128), F32)
    for j in range(2):
        row = jnp.sum(jnp.where(place, level[128 * j : 128 * j + 128], 0.0), axis=0, keepdims=True)
        for k in range(3):
            piece = high(row)
            packed = jnp.where(line == 3 * j + k, piece, packed)
            row = row - piece
    out[128:136, :] = packed.astype(BF)


def merge_kernel(parts, w_out, out):
    extra = parts[:, 128:136, :].astype(F32)
    factors = []
    for j in range(2):
        level = extra[:, 3 * j, :] + extra[:, 3 * j + 1, :] + extra[:, 3 * j + 2, :]
        weight = jnp.exp(level - jnp.max(level, axis=0, keepdims=True))
        factors.append(weight / jnp.sum(weight, axis=0, keepdims=True))
    factors = jnp.concatenate(factors + [jnp.zeros((96, 128), F32)], axis=0).T
    first = iota((128, 128), 1) < 64
    total = jnp.zeros((128, 128), F32)
    for i in range(16):
        factor = jnp.where(first, factors[:, i : i + 1], factors[:, 16 + i : 17 + i])
        total = total + parts[i, 0:128, :].astype(F32) * factor
    turned = pltpu.roll(total, 64, 1)
    own_lanes = iota((128, 256), 1) // HEAD_DIM == iota((128, 256), 0) % 4
    gather = (iota((32, 128), 1) // 4 == iota((32, 128), 0)).astype(BF)
    attended = []
    for j in range(2):
        half = jnp.where(first, total, turned) if j == 0 else jnp.where(first, turned, total)
        half = jnp.where(own_lanes, jnp.concatenate([half, half], axis=1), 0.0).astype(BF)
        attended.append(dot(gather, half))
    attended = jnp.concatenate(attended, axis=0).astype(BF)
    partial = dot(attended, w_out[...]).astype(BF)
    for i in range(8):
        out[i] = partial


def up_kernel(parts, tokens, gain, w_up, residual_out, out):
    attn = parts[0].astype(F32)
    for i in range(1, 8):
        attn = attn + parts[i].astype(F32)
    residual = (tokens[...].astype(F32) + high(attn)).astype(BF)
    residual_out[...] = residual
    wide = residual.astype(F32)
    squares = jnp.sum(wide * wide, axis=1, keepdims=True)
    squares_high = high(squares)
    row_high = column_to_row(squares_high, 128, 0)
    row_low = column_to_row(squares - squares_high, 128, 0)
    line = iota((8, 128), 0)
    tile = jnp.where(line == 0, row_high, jnp.where(line == 1, row_low, 0.0)).astype(BF)
    normed = (wide * gain[...]).astype(BF)
    for p in range(0, 16, 2):
        up = dot(normed, w_up[:, 128 * p : 128 * p + 256]).astype(BF)
        for k in range(2):
            out[p + k, 0:64, :] = up[:, 128 * k : 128 * k + 128]
            out[p + k, 64:72, :] = tile


def hidden_kernel(parts, out):
    up = parts[0, 0:64, :].astype(F32)
    extra = parts[0, 64:72, :].astype(F32)
    for i in range(1, 16):
        up = up + parts[i, 0:64, :].astype(F32)
        extra = extra + parts[i, 64:72, :].astype(F32)
    squares = row_to_column(extra[0:1] + extra[1:2], 64, 0)
    up = lax.rsqrt(squares / D + EPS) * up
    up = jnp.maximum(up, 0.0)
    hidden = (up * up).astype(BF)
    for i in range(16):
        out[i] = hidden


def down_kernel(parts, w_down, out):
    down = jnp.zeros((64, 256), F32)
    for i in range(0, 16, 2):
        pair = jnp.concatenate([parts[i], parts[i + 1]], axis=1)
        down = down + dot(pair, w_down[128 * i : 128 * i + 256, :])
    down = down.astype(BF)
    for i in range(8):
        out[i] = down


def finish_kernel(parts, residual, out):
    down = parts[0].astype(F32)
    for i in range(1, 8):
        down = down + parts[i].astype(F32)
    out[...] = (residual[...].astype(F32) + high(down)).astype(BF)


def exchange(array, axis):
    return lax.all_to_all(array, axis, split_axis=0, concat_axis=0, tiled=True)


def sent(array, axis):
    return exchange(jnp.broadcast_to(array, (lax.axis_size(axis), *array.shape)), axis)


def shards(
    tokens, mix_gain, w_query, w_key, w_value, w_forget, query_gain,
    key_cache, value_cache, decay_cache, w_out, mlp_gain, w_up, w_down,
):
    shape = jax.ShapeDtypeStruct
    message = call(project_kernel, shape((16, 72, 256), BF), "project")(
        tokens, mix_gain.reshape(1, -1), w_query, w_key.T, w_value.T, w_forget.T
    )
    message = exchange(message, "kv")
    part = call(
        attend_kernel,
        shape((136, 128), BF),
        "attend",
        scratch=[
            pltpu.VMEM((8, 512, 1024), BF),
            pltpu.VMEM((8, 512, 1024), BF),
            pltpu.VMEM((8, 8, 4, 1024), F32),
            pltpu.SemaphoreType.DMA((8,)),
            pltpu.SemaphoreType.DMA((8,)),
            pltpu.SemaphoreType.DMA((8,)),
            pltpu.VMEM((64, 128), F32),
            pltpu.VMEM((256, 128), F32),
            pltpu.VMEM((256, 512), BF),
            pltpu.VMEM((256, 128), F32),
            pltpu.VMEM((256, 128), F32),
            pltpu.VMEM((256, 128), F32),
        ],
        in_specs=[VM, VM, ANY, ANY, ANY],
        limit=40 << 20,
    )(
        message,
        query_gain.reshape(1, -1),
        key_cache.reshape(4096, 1024),
        value_cache.reshape(4096, 1024),
        decay_cache,
    )
    message = call(merge_kernel, shape((8, 64, 256), BF), "merge")(sent(part, "kv"), w_out)
    residual, message = call(up_kernel, (shape((64, 256), BF), shape((16, 72, 128), BF)), "up")(
        exchange(message, "tp"), tokens, mlp_gain.reshape(1, -1), w_up
    )
    message = call(hidden_kernel, shape((16, 64, 128), BF), "hidden")(exchange(message, "kv"))
    message = call(down_kernel, shape((8, 64, 256), BF), "down")(exchange(message, "kv"), w_down)
    return call(finish_kernel, shape((64, 256), BF), "finish")(exchange(message, "tp"), residual)


def solution(mesh):
    return jax.shard_map(
        shards,
        mesh=mesh,
        in_specs=(
            P(None, "kv"),
            P("kv"),
            P("kv", "tp"),
            P("kv", "tp"),
            P("kv", "tp"),
            P("kv", "tp"),
            P(),
            P(None, "tp", None, "kv"),
            P(None, "tp", None, "kv"),
            P(None, "tp", "kv"),
            P("tp", "kv"),
            P("kv"),
            P("kv", "tp"),
            P("tp", "kv"),
        ),
        out_specs=P(None, "kv"),
        check_vma=False,
    )
```

time: 145 us -> 104 us (0.72)
  matrix products: 15.5 us -> 0 us
  waiting for transfers between devices: 14.4 us -> 0 us
  Pallas kernels: 0 us -> 13.3 us
  blocking collectives: 92.5 us -> 79.5 us
  starting transfers between devices: 7.05 us -> 0 us
  other arithmetic: 5.22 us -> 0 us
    all_gather x2 -> x0, blocking collectives: 20.5 us -> none  [gathered_once(): both, at, found = (lax.all_gather(jnp.concatenate(lines), axis), 0, {})]
    dot_general x10 -> x0, matrix products: 15.5 us -> none  [the longest x1 5.74 us: shards(): jnp.einsum('bgjp,bgdp->bgjd', weights.astype(jnp.bfloat16), value_cache,...]
    all_to_all x2 -> x0, waiting for transfers between devices: 14.4 us -> none  [sum_at_owner(): lax.all_to_all(cut_along(array, dim, length), axis, 0, 0, tiled=True)]
    pallas_call x0 -> x7, Pallas kernels: none -> 13.3 us  [run(): pl.pallas_call(kernel, out_shape=outs, in_specs=in_specs or [VM] * len(ar...]
    unnamed x23 -> x28, local copies, waits for them, and re-layouts: 0.65 us -> 9.82 us
    all_to_all x4 -> x6, blocking collectives: 72.1 us -> 79.5 us  [exchange(): return lax.all_to_all(array, axis, split_axis=0, concat_axis=0, tiled=True)]
    all_to_all x2 -> x0, starting transfers between devices: 7.05 us -> none  [sum_at_owner(): lax.all_to_all(cut_along(array, dim, length), axis, 0, 0, tiled=True)]
    reduce_sum x9 -> x0, other arithmetic: 2.94 us -> none  [the longest x1 1 us: over_copies(): return sent_to_all(array, axis).sum(axis=0)]
  transfers between devices with their start and end apart: 2 -> 0, of which waited for: 2 -> 0; matrix products, arithmetic and copies ran while one was open for 1% -> 0% of each run, Pallas kernels for 0% -> 0%
where the time goes in v1:
time: 104 us; the launch traced here: 103 us
  blocking collectives  79.5 us (76%)
  Pallas kernels  13.3 us (13%)
  local copies, waits for them, and re-layouts  9.89 us (10%)
    all_to_all x6, blocking collectives, exchange(): return lax.all_to_all(array, axis, split_axis=0, concat_axis=0, tiled=True)  79.5 us
    pallas_call x7, Pallas kernels, run(): pl.pallas_call(kernel, out_shape=outs, in_specs=in_specs or [VM] * len(ar...  13.3 us
    unnamed x28, local copies, waits for them, and re-layouts  9.82 us

profile of v1, /device:TPU:1, one launch (start us, length us, event | category | flops | bytes accessed | tf_op | source)
XLA Modules:
  0.0 102.9 jit_solution(17389488117523967105)
XLA Ops:
  0.0 0.9 copy-done.4
  0.9 0.8 copy-done.5
  1.7 0.8 copy-done.8
  2.4 0.8 copy-done.9
  3.2 0.7 copy-done.10
  3.9 0.7 copy-done.11
  4.5 0.2 project.1
  4.7 19.7 %all_to_all.30.parts = bf16[16,72,256]{2,1,0:T(8,128)(2,1)S(1)} all-to-all(bf16[16,72,256]{2,1,0:T(8,128)(2,1)S(1)} %project.1), channel_id=1, replica_groups=mesh['kv'=16,'tp'=8] {'kv'}, dimensions={0} | all-to-all | bytes 1179648 | tf_op jit(solution)/shard_map/all_to_all | solution.py:275
  24.5 3.4 %copy-done = bf16[64,1,64,1024]{3,2,1,0:T(8,128)(2,1)S(1)} copy-done((bf16[64,1,64,1024]{3,2,1,0:T(8,128)(2,1)S(1)}, bf16[64,1,64,1024]{3,2,1,0:T(8,128)(2,1)}, u32[]{:S(2)}) %copy-start) | copy-done | bytes 8388632
  27.8 1.2 %copy-done.1 = f32[64,4,1024]{2,1,0:T(4,128)S(1)} copy-done((f32[64,4,1024]{2,1,0:T(4,128)S(1)}, f32[64,4,1024]{2,1,0:T(4,128)}, u32[]{:S(2)}) %copy-start.1) | copy-done | bytes 1048600
  29.1 0.7 copy-done.13
  29.7 0.0 copy-start.2
  29.7 10.5 %attend.1 = bf16[136,128]{1,0:T(8,128)(2,1)S(1)} custom-call(bf16[16,72,256]{2,1,0:T(8,128)(2,1)S(1)} %all_to_all.30.parts, f32[1,64]{1,0:T(1,128)S(1)} %bitcast.14, bf16[4096,1024]{1,0:T(8,128)(2,1)S(1)} %bitcast.8, bf16[4096,1024]{1,0:T(8,128)(2,1)} %bitcast.15, f32[64,4,1024]{2,1,0:T(4,128)S(1)} %copy-done.1), custom_call_target="tpu_custom_call" | custom-call | tf_op jit(solution)/shard_map/attend/pallas_call | solution.py:50
  40.3 0.1 broadcast_in_dim.3
  40.3 13.2 %all_to_all.31.parts = bf16[16,136,128]{2,1,0:T(8,128)(2,1)S(1)} all-to-all(bf16[16,136,128]{2,1,0:T(8,128)(2,1)S(1)} %broadcast_in_dim.3), channel_id=1, replica_groups=mesh['kv'=16,'tp'=8] {'kv'}, dimensions={0} | all-to-all | bytes 1114112 | tf_op jit(solution)/shard_map/all_to_all | solution.py:275
  53.5 1.2 %merge.1 = bf16[8,64,256]{2,1,0:T(8,128)(2,1)S(1)} custom-call(bf16[16,136,128]{2,1,0:T(8,128)(2,1)S(1)} %all_to_all.31.parts, bf16[256,256]{1,0:T(8,128)(2,1)S(1)} %copy-done.7), custom_call_target="tpu_custom_call" | custom-call | tf_op jit(solution)/shard_map/merge/pallas_call | solution.py:50
  54.8 13.2 %all_to_all.32.parts = bf16[8,64,256]{2,1,0:T(8,128)(2,1)S(1)} all-to-all(bf16[8,64,256]{2,1,0:T(8,128)(2,1)S(1)} %merge.1), channel_id=1, replica_groups=mesh['kv'=16,'tp'=8] {'tp'}, dimensions={0} | all-to-all | bytes 524288 | tf_op jit(solution)/shard_map/all_to_all | solution.py:275
  68.0 0.3 up.1
  68.4 10.7 %all_to_all.33.parts = bf16[16,72,128]{2,1,0:T(8,128)(2,1)S(1)} all-to-all(bf16[16,72,128]{2,1,0:T(8,128)(2,1)S(1)} %get-tuple-element.7), channel_id=1, replica_groups=mesh['kv'=16,'tp'=8] {'kv'}, dimensions={0} | all-to-all | bytes 589824 | tf_op jit(solution)/shard_map/all_to_all | solution.py:275
  79.0 0.1 hidden.1
  79.2 10.2 %all_to_all.34.parts = bf16[16,64,128]{2,1,0:T(8,128)(2,1)S(1)} all-to-all(bf16[16,64,128]{2,1,0:T(8,128)(2,1)S(1)} %hidden.1), channel_id=1, replica_groups=mesh['kv'=16,'tp'=8] {'kv'}, dimensions={0} | all-to-all | bytes 524288 | tf_op jit(solution)/shard_map/all_to_all | solution.py:275
  89.4 0.3 down.1
  89.7 12.5 %all_to_all.35.parts = bf16[8,64,256]{2,1,0:T(8,128)(2,1)S(1)} all-to-all(bf16[8,64,256]{2,1,0:T(8,128)(2,1)S(1)} %down.1), channel_id=1, replica_groups=mesh['kv'=16,'tp'=8] {'tp'}, dimensions={0} | all-to-all | bytes 524288 | tf_op jit(solution)/shard_map/all_to_all | solution.py:275
  102.2 0.7 finish.1
  (18 shorter events, 0.0 us)
Async XLA Ops:
  0.0 0.9 copy-start.4
  0.9 0.8 copy-start.5
  1.7 0.8 copy-start.8
  2.4 0.8 copy-start.9
  3.2 0.7 copy-start.10
  3.9 0.7 copy-start.11
  24.5 3.4 %copy-start = (bf16[64,1,64,1024]{3,2,1,0:T(8,128)(2,1)S(1)}, bf16[64,1,64,1024]{3,2,1,0:T(8,128)(2,1)}, u32[]{:S(2)}) copy-start(bf16[64,1,64,1024]{3,2,1,0:T(8,128)(2,1)} %param.21) | copy-start | bytes 25165828
  27.8 1.2 %copy-start.1 = (f32[64,4,1024]{2,1,0:T(4,128)S(1)}, f32[64,4,1024]{2,1,0:T(4,128)}, u32[]{:S(2)}) copy-start(f32[64,4,1024]{2,1,0:T(4,128)} %decay_hbm.1) | copy-start | bytes 3145732
  29.1 0.7 copy-start.13
  29.7 23.8 %copy-start.7 = (bf16[256,256]{1,0:T(8,128)(2,1)S(1)}, bf16[256,256]{1,0:T(8,128)(2,1)}, u32[]{:S(2)}) copy-start(bf16[256,256]{1,0:T(8,128)(2,1)} %w_out.1) | copy-start | bytes 393220
  29.7 38.3 %copy-start.3 = (bf16[256,2048]{1,0:T(8,128)(2,1)S(1)}, bf16[256,2048]{1,0:T(8,128)(2,1)}, u32[]{:S(2)}) copy-start(bf16[256,2048]{1,0:T(8,128)(2,1)} %w_up.1) | copy-start | bytes 3145732
  29.7 38.3 %copy-start.6 = (bf16[64,256]{1,0:T(8,128)(2,1)S(1)}, bf16[64,256]{1,0:T(8,128)(2,1)}, u32[]{:S(2)}) copy-start(bf16[64,256]{1,0:T(8,128)(2,1)} %tokens.3) | copy-start | bytes 98308
  29.7 38.3 %copy-start.12 = (f32[256]{0:T(256)S(1)}, f32[256]{0:T(256)}, u32[]{:S(2)}) copy-start(f32[256]{0:T(256)} %param.25) | copy-start | bytes 3076
  29.7 59.7 %copy-start.2 = (bf16[2048,256]{1,0:T(8,128)(2,1)S(1)}, bf16[2048,256]{1,0:T(8,128)(2,1)}, u32[]{:S(2)}) copy-start(bf16[2048,256]{1,0:T(8,128)(2,1)} %w_down.1) | copy-start | bytes 3145732

commit v2 on v1

--- a/solution.py
+++ b/solution.py
@@ -14,7 +14,7 @@
 F32 = jnp.float32
 
 VM = pl.BlockSpec(memory_space=pltpu.VMEM)
-ANY = pl.BlockSpec(memory_space=pl.ANY)
+HBM = pl.BlockSpec(memory_space=pltpu.HBM)
 
 
 def iota(shape, dim):
@@ -45,7 +45,7 @@
     return jnp.sum(jnp.where(place, row, 0.0), axis=1, keepdims=True)
 
 
-def call(kernel, outs, name, scratch=(), in_specs=None, limit=16 << 20):
+def call(kernel, outs, name, scratch=(), in_specs=None, limit=16 << 20, cost=None):
     def run(*args):
         return pl.pallas_call(
             kernel,
@@ -55,16 +55,24 @@
             scratch_shapes=list(scratch),
             compiler_params=pltpu.CompilerParams(vmem_limit_bytes=limit),
             name=name,
+            cost_estimate=cost and pl.CostEstimate(flops=cost, bytes_accessed=cost // 100, transcendentals=0),
         )(*args)
 
     return run
 
 
-def project_kernel(tokens, gain, w_query, w_key, w_value, w_forget, out):
+def project_kernel(*refs):
+    sources, (query_out, extra_out), held, sem = refs[:6], refs[6:8], refs[8:14], refs[14]
+    copies = [pltpu.make_async_copy(s, h, sem.at[k]) for k, (s, h) in enumerate(zip(sources, held))]
+    for copy in copies:
+        copy.start()
+    for copy in copies:
+        copy.wait()
+    tokens, gain, w_query, w_key, w_value, w_forget = held
     stream = tokens[...].astype(F32)
     squares = jnp.sum(stream * stream, axis=1, keepdims=True)
     normed = (stream * gain[...]).astype(BF)
-    query = dot(normed, w_query[...]).astype(BF)
+    query_out[...] = dot(normed, w_query[...]).astype(BF)
     key_value = dot_t(normed, jnp.concatenate([w_key[...], w_value[...]], axis=0))
     forget_w = w_forget[...].astype(F32)
     forget_w = jnp.concatenate([forget_w, forget_w, jnp.zeros((120, 256), F32)], axis=0)
@@ -73,30 +81,22 @@
     squares_high = high(squares)
     row_high = column_to_row(squares_high, 128, 64)
     row_low = column_to_row(squares - squares_high, 128, 64)
-    line = iota((8, 128), 0)
-    square_tile = jnp.where(line == 0, row_high, jnp.where(line == 1, row_low, 0.0))
+    line = iota((64, 128), 0) % 8
+    forget = forget + jnp.where(line == 0, row_high, jnp.where(line == 1, row_low, 0.0))
+    extra_out[:, 0:128] = key_value.astype(BF)
+    extra_out[:, 128:256] = forget.astype(BF)
+
+
+def spread_kernel(query, extra, out):
     for p in range(16):
-        t = p // 2
-        out[p, 0:64, :] = query
-        out[p, 64:72, 0:128] = key_value[8 * t : 8 * t + 8].astype(BF)
-        out[p, 64:72, 128:256] = (forget[8 * t : 8 * t + 8] + square_tile).astype(BF)
+        out[p, 0:64, :] = query[...]
+        out[p, 64:72, :] = extra[8 * (p // 2) : 8 * (p // 2) + 8, :]
 
 
 def attend_kernel(
-    parts, query_gain, key_hbm, value_hbm, decay_hbm, out,
-    keys, values, decay, key_sem, value_sem, decay_sem, scales, query_rows, left, peaks, masses, sums,
+    parts, query_gain, keys, values, decay, out,
+    scales, query_rows, left, peaks, masses, sums,
 ):
-    copies = []
-    for g in range(8):
-        rows = pl.ds(512 * g, 512)
-        k_copy = pltpu.make_async_copy(key_hbm.at[rows], keys.at[g], key_sem.at[g])
-        d_copy = pltpu.make_async_copy(decay_hbm.at[pl.ds(8 * g, 8)], decay.at[g], decay_sem.at[g])
-        v_copy = pltpu.make_async_copy(value_hbm.at[rows], values.at[g], value_sem.at[g])
-        k_copy.start()
-        d_copy.start()
-        v_copy.start()
-        copies.append((k_copy, d_copy, v_copy))
-
     raw = parts[0, 0:64, :].astype(F32)
     extra = parts[0, 64:72, :].astype(F32)
     for i in range(1, 16):
@@ -129,17 +129,13 @@
 
     diagonal = iota((32, 512), 1) // HEAD_DIM == iota((32, 512), 0) // 4
     for g in range(8):
-        k_copy, d_copy, v_copy = copies[g]
         rows = slice(32 * g, 32 * g + 32)
-        k_copy.wait()
-        scores = dot(left[rows, :], keys[g]) * (HEAD_DIM ** (-0.5))
-        d_copy.wait()
-        scores = scores + decay[g].reshape(32, 1024)
+        scores = dot(left[rows, :], keys[512 * g : 512 * g + 512, :]) * (HEAD_DIM ** (-0.5))
+        scores = scores + decay[8 * g : 8 * g + 8].reshape(32, 1024)
         peak = jnp.max(scores, axis=1, keepdims=True)
         weights = jnp.exp(scores - peak)
         mass = jnp.sum(weights, axis=1, keepdims=True)
-        v_copy.wait()
-        summed = dot_t(weights.astype(BF), values[g])
+        summed = dot_t(weights.astype(BF), values[512 * g : 512 * g + 512, :])
         summed = jnp.where(diagonal, summed, 0.0)
         summed = (summed[:, 0:128] + summed[:, 128:256]) + (summed[:, 256:384] + summed[:, 384:512])
         sums[rows, :] = summed + pltpu.roll(summed, 64, 1)
@@ -284,21 +280,28 @@
     key_cache, value_cache, decay_cache, w_out, mlp_gain, w_up, w_down,
 ):
     shape = jax.ShapeDtypeStruct
-    message = call(project_kernel, shape((16, 72, 256), BF), "project")(
-        tokens, mix_gain.reshape(1, -1), w_query, w_key.T, w_value.T, w_forget.T
-    )
+    query, extra = call(
+        project_kernel,
+        (shape((64, 256), BF), shape((64, 256), BF)),
+        "project",
+        scratch=[
+            pltpu.VMEM((64, 256), BF),
+            pltpu.VMEM((1, 256), F32),
+            pltpu.VMEM((256, 256), BF),
+            pltpu.VMEM((64, 256), BF),
+            pltpu.VMEM((64, 256), BF),
+            pltpu.VMEM((4, 256), BF),
+            pltpu.SemaphoreType.DMA((6,)),
+        ],
+        in_specs=[HBM] * 6,
+    )(tokens, mix_gain.reshape(1, -1), w_query, w_key.T, w_value.T, w_forget.T)
+    message = call(spread_kernel, shape((16, 72, 256), BF), "spread", cost=10**10)(query, extra)
     message = exchange(message, "kv")
     part = call(
         attend_kernel,
         shape((136, 128), BF),
         "attend",
         scratch=[
-            pltpu.VMEM((8, 512, 1024), BF),
-            pltpu.VMEM((8, 512, 1024), BF),
-            pltpu.VMEM((8, 8, 4, 1024), F32),
-            pltpu.SemaphoreType.DMA((8,)),
-            pltpu.SemaphoreType.DMA((8,)),
-            pltpu.SemaphoreType.DMA((8,)),
             pltpu.VMEM((64, 128), F32),
             pltpu.VMEM((256, 128), F32),
             pltpu.VMEM((256, 512), BF),
@@ -306,8 +309,8 @@
             pltpu.VMEM((256, 128), F32),
             pltpu.VMEM((256, 128), F32),
         ],
-        in_specs=[VM, VM, ANY, ANY, ANY],
-        limit=40 << 20,
+
+        limit=8 << 20,
     )(
         message,
         query_gain.reshape(1, -1),

time: 104 us -> 94 us (0.904)
  local copies, waits for them, and re-layouts: 9.89 us -> 4.67 us
  Pallas kernels: 13.3 us -> 8.87 us
    unnamed x28 -> x30, local copies, waits for them, and re-layouts: 9.82 us -> 4.59 us
    pallas_call x7 -> x8, Pallas kernels: 13.3 us -> 8.87 us  [run(): pl.pallas_call(kernel, out_shape=outs, in_specs=in_specs or [VM] * len(ar...]
where the time goes in v2:
time: 94 us; the launch traced here: 93.5 us
  blocking collectives  79.8 us (85%)
  Pallas kernels  8.87 us (9%)
  local copies, waits for them, and re-layouts  4.67 us (5%)
    all_to_all x6, blocking collectives, exchange(): return lax.all_to_all(array, axis, split_axis=0, concat_axis=0, tiled=True)  79.8 us
    pallas_call x8, Pallas kernels, run(): pl.pallas_call(kernel, out_shape=outs, in_specs=in_specs or [VM] * len(ar...  8.87 us
    unnamed x30, local copies, waits for them, and re-layouts  4.59 us

profile of v2, /device:TPU:1, one launch (start us, length us, event | category | flops | bytes accessed | tf_op | source)
XLA Modules:
  0.0 93.5 jit_solution(16934386047119814880)
XLA Ops:
  0.0 0.8 copy-done.5
  0.8 0.9 copy-done.7
  1.7 0.8 copy-done.9
  2.4 0.8 copy-done.10
  3.2 0.7 copy-done.11
  3.9 0.7 copy-done.12
  4.5 0.5 project.1
  5.1 0.0 copy-start
  5.1 0.0 copy-start.1
  5.2 20.0 %all_to_all.30.parts = bf16[16,72,256]{2,1,0:T(8,128)(2,1)S(1)} all-to-all(bf16[16,72,256]{2,1,0:T(8,128)(2,1)S(1)} %spread.1), channel_id=1, replica_groups=mesh['kv'=16,'tp'=8] {'kv'}, dimensions={0} | all-to-all | bytes 1179648 | tf_op jit(solution)/shard_map/all_to_all | solution.py:271
  25.1 0.0 copy-start.8
  25.2 0.0 copy-start.13
  25.2 5.7 %attend.1 = bf16[136,128]{1,0:T(8,128)(2,1)S(1)} custom-call(bf16[16,72,256]{2,1,0:T(8,128)(2,1)S(1)} %all_to_all.30.parts, f32[1,64]{1,0:T(1,128)S(1)} %bitcast.15, bf16[4096,1024]{1,0:T(8,128)(2,1)S(1)} %bitcast.8, bf16[4096,1024]{1,0:T(8,128)(2,1)S(1)} %bitcast.9, f32[64,4,1024]{2,1,0:T(4,128)S(1)} %copy-done.2), custom_call_target="tpu_custom_call" | custom-call | tf_op jit(solution)/shard_map/attend/pallas_call | solution.py:50
  30.9 0.1 broadcast_in_dim.3
  31.0 13.2 %all_to_all.31.parts = bf16[16,136,128]{2,1,0:T(8,128)(2,1)S(1)} all-to-all(bf16[16,136,128]{2,1,0:T(8,128)(2,1)S(1)} %broadcast_in_dim.3), channel_id=1, replica_groups=mesh['kv'=16,'tp'=8] {'kv'}, dimensions={0} | all-to-all | bytes 1114112 | tf_op jit(solution)/shard_map/all_to_all | solution.py:271
  44.2 1.2 %merge.1 = bf16[8,64,256]{2,1,0:T(8,128)(2,1)S(1)} custom-call(bf16[16,136,128]{2,1,0:T(8,128)(2,1)S(1)} %all_to_all.31.parts, bf16[256,256]{1,0:T(8,128)(2,1)S(1)} %copy-done.8), custom_call_target="tpu_custom_call" | custom-call | tf_op jit(solution)/shard_map/merge/pallas_call | solution.py:50
  45.4 13.2 %all_to_all.32.parts = bf16[8,64,256]{2,1,0:T(8,128)(2,1)S(1)} all-to-all(bf16[8,64,256]{2,1,0:T(8,128)(2,1)S(1)} %merge.1), channel_id=1, replica_groups=mesh['kv'=16,'tp'=8] {'tp'}, dimensions={0} | all-to-all | bytes 524288 | tf_op jit(solution)/shard_map/all_to_all | solution.py:271
  58.7 0.3 up.1
  59.0 10.7 %all_to_all.33.parts = bf16[16,72,128]{2,1,0:T(8,128)(2,1)S(1)} all-to-all(bf16[16,72,128]{2,1,0:T(8,128)(2,1)S(1)} %get-tuple-element.11), channel_id=1, replica_groups=mesh['kv'=16,'tp'=8] {'kv'}, dimensions={0} | all-to-all | bytes 589824 | tf_op jit(solution)/shard_map/all_to_all | solution.py:271
  69.7 0.1 hidden.1
  69.8 10.2 %all_to_all.34.parts = bf16[16,64,128]{2,1,0:T(8,128)(2,1)S(1)} all-to-all(bf16[16,64,128]{2,1,0:T(8,128)(2,1)S(1)} %hidden.1), channel_id=1, replica_groups=mesh['kv'=16,'tp'=8] {'kv'}, dimensions={0} | all-to-all | bytes 524288 | tf_op jit(solution)/shard_map/all_to_all | solution.py:271
  80.1 0.3 down.1
  80.4 12.5 %all_to_all.35.parts = bf16[8,64,256]{2,1,0:T(8,128)(2,1)S(1)} all-to-all(bf16[8,64,256]{2,1,0:T(8,128)(2,1)S(1)} %down.1), channel_id=1, replica_groups=mesh['kv'=16,'tp'=8] {'tp'}, dimensions={0} | all-to-all | bytes 524288 | tf_op jit(solution)/shard_map/all_to_all | solution.py:271
  92.8 0.7 finish.1
  (21 shorter events, 0.1 us)
Async XLA Ops:
  0.0 0.8 copy-start.5
  0.8 0.9 copy-start.7
  1.7 0.8 copy-start.9
  2.4 0.8 copy-start.10
  3.2 0.7 copy-start.11
  3.9 0.7 copy-start.12
  5.1 20.1 %copy-start = (bf16[64,1,64,1024]{3,2,1,0:T(8,128)(2,1)S(1)}, bf16[64,1,64,1024]{3,2,1,0:T(8,128)(2,1)}, u32[]{:S(2)}) copy-start(bf16[64,1,64,1024]{3,2,1,0:T(8,128)(2,1)} %param.21) | copy-start | bytes 25165828
  5.1 20.1 %copy-start.1 = (bf16[64,1,64,1024]{3,2,1,0:T(8,128)(2,1)S(1)}, bf16[64,1,64,1024]{3,2,1,0:T(8,128)(2,1)}, u32[]{:S(2)}) copy-start(bf16[64,1,64,1024]{3,2,1,0:T(8,128)(2,1)} %param.22) | copy-start | bytes 25165828
  5.1 20.1 %copy-start.2 = (f32[64,4,1024]{2,1,0:T(4,128)S(1)}, f32[64,4,1024]{2,1,0:T(4,128)}, u32[]{:S(2)}) copy-start(f32[64,4,1024]{2,1,0:T(4,128)} %decay.1) | copy-start | bytes 3145732
  5.1 20.0 %copy-start.14 = (f32[64]{0:T(128)S(1)}, f32[64]{0:T(128)}, u32[]{:S(2)}) copy-start(f32[64]{0:T(128)} %param.20) | copy-start | bytes 772
  25.1 19.0 %copy-start.8 = (bf16[256,256]{1,0:T(8,128)(2,1)S(1)}, bf16[256,256]{1,0:T(8,128)(2,1)}, u32[]{:S(2)}) copy-start(bf16[256,256]{1,0:T(8,128)(2,1)} %w_out.1) | copy-start | bytes 393220
  25.2 33.5 %copy-start.4 = (bf16[256,2048]{1,0:T(8,128)(2,1)S(1)}, bf16[256,2048]{1,0:T(8,128)(2,1)}, u32[]{:S(2)}) copy-start(bf16[256,2048]{1,0:T(8,128)(2,1)} %w_up.1) | copy-start | bytes 3145732
  25.2 33.5 %copy-start.6 = (bf16[64,256]{1,0:T(8,128)(2,1)S(1)}, bf16[64,256]{1,0:T(8,128)(2,1)}, u32[]{:S(2)}) copy-start(bf16[64,256]{1,0:T(8,128)(2,1)} %tokens.1) | copy-start | bytes 98308
  25.2 33.5 %copy-start.13 = (f32[256]{0:T(256)S(1)}, f32[256]{0:T(256)}, u32[]{:S(2)}) copy-start(f32[256]{0:T(256)} %param.25) | copy-start | bytes 3076
  25.2 54.9 %copy-start.3 = (bf16[2048,256]{1,0:T(8,128)(2,1)S(1)}, bf16[2048,256]{1,0:T(8,128)(2,1)}, u32[]{:S(2)}) copy-start(bf16[2048,256]{1,0:T(8,128)(2,1)} %w_down.1) | copy-start | bytes 3145732

commit v3 on v2

--- a/solution.py
+++ b/solution.py
@@ -14,7 +14,6 @@
 F32 = jnp.float32
 
 VM = pl.BlockSpec(memory_space=pltpu.VMEM)
-HBM = pl.BlockSpec(memory_space=pltpu.HBM)
 
 
 def iota(shape, dim):
@@ -61,14 +60,7 @@
     return run
 
 
-def project_kernel(*refs):
-    sources, (query_out, extra_out), held, sem = refs[:6], refs[6:8], refs[8:14], refs[14]
-    copies = [pltpu.make_async_copy(s, h, sem.at[k]) for k, (s, h) in enumerate(zip(sources, held))]
-    for copy in copies:
-        copy.start()
-    for copy in copies:
-        copy.wait()
-    tokens, gain, w_query, w_key, w_value, w_forget = held
+def project_kernel(head, tokens, gain, w_query, w_key, w_value, w_forget, query_out, extra_out):
     stream = tokens[...].astype(F32)
     squares = jnp.sum(stream * stream, axis=1, keepdims=True)
     normed = (stream * gain[...]).astype(BF)
@@ -85,6 +77,10 @@
     forget = forget + jnp.where(line == 0, row_high, jnp.where(line == 1, row_low, 0.0))
     extra_out[:, 0:128] = key_value.astype(BF)
     extra_out[:, 128:256] = forget.astype(BF)
+
+
+def head_kernel(out):
+    out[...] = jnp.zeros_like(out)
 
 
 def spread_kernel(query, extra, out):
@@ -280,21 +276,9 @@
     key_cache, value_cache, decay_cache, w_out, mlp_gain, w_up, w_down,
 ):
     shape = jax.ShapeDtypeStruct
-    query, extra = call(
-        project_kernel,
-        (shape((64, 256), BF), shape((64, 256), BF)),
-        "project",
-        scratch=[
-            pltpu.VMEM((64, 256), BF),
-            pltpu.VMEM((1, 256), F32),
-            pltpu.VMEM((256, 256), BF),
-            pltpu.VMEM((64, 256), BF),
-            pltpu.VMEM((64, 256), BF),
-            pltpu.VMEM((4, 256), BF),
-            pltpu.SemaphoreType.DMA((6,)),
-        ],
-        in_specs=[HBM] * 6,
-    )(tokens, mix_gain.reshape(1, -1), w_query, w_key.T, w_value.T, w_forget.T)
+    head = call(head_kernel, shape((8, 128), F32), "head", cost=3 * 10**9)()
+    operands = (tokens, mix_gain.reshape(1, -1), w_query, w_key.T, w_value.T, w_forget.T)
+    query, extra = call(project_kernel, (shape((64, 256), BF), shape((64, 256), BF)), "project")(head, *operands)
     message = call(spread_kernel, shape((16, 72, 256), BF), "spread", cost=10**10)(query, extra)
     message = exchange(message, "kv")
     part = call(

time: 94 us -> 89.9 us (0.956)
  local copies, waits for them, and re-layouts: 4.67 us -> 1.06 us
    unnamed x30 -> x32, local copies, waits for them, and re-layouts: 4.59 us -> 0.98 us
    pallas_call x8 -> x9, Pallas kernels: 8.87 us -> 8.55 us  [run(): pl.pallas_call(kernel, out_shape=outs, in_specs=in_specs or [VM] * len(ar...]
where the time goes in v3:
time: 89.9 us; the launch traced here: 89.6 us
  blocking collectives  79.8 us (89%)
  Pallas kernels  8.55 us (10%)
  local copies, waits for them, and re-layouts  1.06 us (1%)
    all_to_all x6, blocking collectives, exchange(): return lax.all_to_all(array, axis, split_axis=0, concat_axis=0, tiled=True)  79.8 us
    pallas_call x9, Pallas kernels, run(): pl.pallas_call(kernel, out_shape=outs, in_specs=in_specs or [VM] * len(ar...  8.55 us

profile of v3, /device:TPU:1, one launch (start us, length us, event | category | flops | bytes accessed | tf_op | source)
XLA Modules:
  0.0 89.6 jit_solution(2278802552586034972)
XLA Ops:
  0.0 0.0 slice-start
  0.1 0.0 slice-start.2
  0.1 0.7 copy-done.4
  0.8 0.0 copy-done.7
  0.8 0.0 copy-done.6
  0.8 0.2 copy-done.3
  1.0 0.2 project.1
  1.2 0.0 slice-start.1
  1.2 0.0 slice-start.3
  1.2 0.0 copy-start.11
  1.3 20.0 %all_to_all.30.parts = bf16[16,72,256]{2,1,0:T(8,128)(2,1)S(1)} all-to-all(bf16[16,72,256]{2,1,0:T(8,128)(2,1)S(1)} %spread.1), channel_id=1, replica_groups=mesh['kv'=16,'tp'=8] {'kv'}, dimensions={0} | all-to-all | bytes 1179648 | tf_op jit(solution)/shard_map/all_to_all | solution.py:267
  21.3 0.0 copy-start.2
  21.4 5.7 %attend.1 = bf16[136,128]{1,0:T(8,128)(2,1)S(1)} custom-call(bf16[16,72,256]{2,1,0:T(8,128)(2,1)S(1)} %all_to_all.30.parts, f32[1,64]{1,0:T(1,128)S(1)} %bitcast.19, bf16[4096,1024]{1,0:T(8,128)(2,1)S(1)} %bitcast.10, bf16[4096,1024]{1,0:T(8,128)(2,1)S(1)} %bitcast.13, f32[64,4,1024]{2,1,0:T(4,128)S(1)} %copy-done), custom_call_target="tpu_custom_call" | custom-call | tf_op jit(solution)/shard_map/attend/pallas_call | solution.py:49
  27.1 0.1 broadcast_in_dim.3
  27.1 13.2 %all_to_all.31.parts = bf16[16,136,128]{2,1,0:T(8,128)(2,1)S(1)} all-to-all(bf16[16,136,128]{2,1,0:T(8,128)(2,1)S(1)} %broadcast_in_dim.3), channel_id=1, replica_groups=mesh['kv'=16,'tp'=8] {'kv'}, dimensions={0} | all-to-all | bytes 1114112 | tf_op jit(solution)/shard_map/all_to_all | solution.py:267
  40.4 1.2 %merge.1 = bf16[8,64,256]{2,1,0:T(8,128)(2,1)S(1)} custom-call(bf16[16,136,128]{2,1,0:T(8,128)(2,1)S(1)} %all_to_all.31.parts, bf16[256,256]{1,0:T(8,128)(2,1)S(1)} %copy-done.5), custom_call_target="tpu_custom_call" | custom-call | tf_op jit(solution)/shard_map/merge/pallas_call | solution.py:49
  41.6 13.2 %all_to_all.32.parts = bf16[8,64,256]{2,1,0:T(8,128)(2,1)S(1)} all-to-all(bf16[8,64,256]{2,1,0:T(8,128)(2,1)S(1)} %merge.1), channel_id=1, replica_groups=mesh['kv'=16,'tp'=8] {'tp'}, dimensions={0} | all-to-all | bytes 524288 | tf_op jit(solution)/shard_map/all_to_all | solution.py:267
  54.8 0.3 up.1
  55.1 10.7 %all_to_all.33.parts = bf16[16,72,128]{2,1,0:T(8,128)(2,1)S(1)} all-to-all(bf16[16,72,128]{2,1,0:T(8,128)(2,1)S(1)} %get-tuple-element.11), channel_id=1, replica_groups=mesh['kv'=16,'tp'=8] {'kv'}, dimensions={0} | all-to-all | bytes 589824 | tf_op jit(solution)/shard_map/all_to_all | solution.py:267
  65.8 0.1 hidden.1
  65.9 10.2 %all_to_all.34.parts = bf16[16,64,128]{2,1,0:T(8,128)(2,1)S(1)} all-to-all(bf16[16,64,128]{2,1,0:T(8,128)(2,1)S(1)} %hidden.1), channel_id=1, replica_groups=mesh['kv'=16,'tp'=8] {'kv'}, dimensions={0} | all-to-all | bytes 524288 | tf_op jit(solution)/shard_map/all_to_all | solution.py:267
  76.2 0.3 down.1
  76.5 12.5 %all_to_all.35.parts = bf16[8,64,256]{2,1,0:T(8,128)(2,1)S(1)} all-to-all(bf16[8,64,256]{2,1,0:T(8,128)(2,1)S(1)} %down.1), channel_id=1, replica_groups=mesh['kv'=16,'tp'=8] {'tp'}, dimensions={0} | all-to-all | bytes 524288 | tf_op jit(solution)/shard_map/all_to_all | solution.py:267
  89.0 0.7 finish.1
  (26 shorter events, 0.1 us)
Async XLA Ops:
  0.0 0.8 copy-start.4
  0.0 0.8 copy-start.8
  0.0 0.8 copy-start.7
  0.0 0.8 copy-start.6
  0.0 1.0 %copy-start.3 = (bf16[256,256]{1,0:T(8,128)(2,1)S(1)}, bf16[256,256]{1,0:T(8,128)(2,1)}, u32[]{:S(2)}) copy-start(bf16[256,256]{1,0:T(8,128)(2,1)} %w_query.1) | copy-start | bytes 393220
  0.0 1.0 %copy-start.10 = (f32[256]{0:T(256)S(1)}, f32[256]{0:T(256)}, u32[]{:S(2)}) copy-start(f32[256]{0:T(256)} %param.15) | copy-start | bytes 3076
  0.0 21.2 %slice-start = ((s8[8388608]{0:T(1024)(128)(4,1)}), s8[4194304]{0:T(1024)(128)(4,1)S(1)}, s32[]{:S(2)}) async-start(s8[8388608]{0:T(1024)(128)(4,1)} %bitcast.8), calls=%async_computation.6 | async-start | bytes 8388608
  0.1 21.2 %slice-start.2 = ((s8[8388608]{0:T(1024)(128)(4,1)}), s8[4194304]{0:T(1024)(128)(4,1)S(1)}, s32[]{:S(2)}) async-start(s8[8388608]{0:T(1024)(128)(4,1)} %bitcast.11), calls=%async_computation.8 | async-start | bytes 8388608
  1.2 20.1 %slice-start.1 = ((s8[8388608]{0:T(1024)(128)(4,1)}), s8[4194304]{0:T(1024)(128)(4,1)S(1)}, s32[]{:S(2)}) async-start(s8[8388608]{0:T(1024)(128)(4,1)} %bitcast.8), calls=%async_computation.7 | async-start | bytes 8388608
  1.2 20.1 %slice-start.3 = ((s8[8388608]{0:T(1024)(128)(4,1)}), s8[4194304]{0:T(1024)(128)(4,1)S(1)}, s32[]{:S(2)}) async-start(s8[8388608]{0:T(1024)(128)(4,1)} %bitcast.11), calls=%async_computation.9 | async-start | bytes 8388608
  1.2 20.1 %copy-start = (f32[64,4,1024]{2,1,0:T(4,128)S(1)}, f32[64,4,1024]{2,1,0:T(4,128)}, u32[]{:S(2)}) copy-start(f32[64,4,1024]{2,1,0:T(4,128)} %decay.1) | copy-start | bytes 3145732
  1.2 20.1 %copy-start.11 = (f32[64]{0:T(128)S(1)}, f32[64]{0:T(128)}, u32[]{:S(2)}) copy-start(f32[64]{0:T(128)} %param.20) | copy-start | bytes 772
  21.3 19.1 %copy-start.5 = (bf16[256,256]{1,0:T(8,128)(2,1)S(1)}, bf16[256,256]{1,0:T(8,128)(2,1)}, u32[]{:S(2)}) copy-start(bf16[256,256]{1,0:T(8,128)(2,1)} %w_out.1) | copy-start | bytes 393220
  21.3 33.5 %copy-start.2 = (bf16[256,2048]{1,0:T(8,128)(2,1)S(1)}, bf16[256,2048]{1,0:T(8,128)(2,1)}, u32[]{:S(2)}) copy-start(bf16[256,2048]{1,0:T(8,128)(2,1)} %w_up.1) | copy-start | bytes 3145732
  21.3 33.5 %copy-start.9 = (f32[256]{0:T(256)S(1)}, f32[256]{0:T(256)}, u32[]{:S(2)}) copy-start(f32[256]{0:T(256)} %param.25) | copy-start | bytes 3076
  21.3 54.8 %copy-start.1 = (bf16[2048,256]{1,0:T(8,128)(2,1)S(1)}, bf16[2048,256]{1,0:T(8,128)(2,1)}, u32[]{:S(2)}) copy-start(bf16[2048,256]{1,0:T(8,128)(2,1)} %w_down.1) | copy-start | bytes 3145732

commit v4 on v3

--- a/solution.py
+++ b/solution.py
@@ -91,7 +91,7 @@
 
 def attend_kernel(
     parts, query_gain, keys, values, decay, out,
-    scales, query_rows, left, peaks, masses, sums,
+    scales, query_rows, left, peaks, masses,
 ):
     raw = parts[0, 0:64, :].astype(F32)
     extra = parts[0, 64:72, :].astype(F32)
@@ -123,7 +123,8 @@
     block = iota((256, 512), 1) // HEAD_DIM == (iota((256, 512), 0) // 4) % 8
     left[...] = jnp.where(block, wide, 0.0).astype(BF)
 
-    diagonal = iota((32, 512), 1) // HEAD_DIM == iota((32, 512), 0) // 4
+    lane = iota((64, 128), 1)
+    sums = []
     for g in range(8):
         rows = slice(32 * g, 32 * g + 32)
         scores = dot(left[rows, :], keys[512 * g : 512 * g + 512, :]) * (HEAD_DIM ** (-0.5))
@@ -131,12 +132,15 @@
         peak = jnp.max(scores, axis=1, keepdims=True)
         weights = jnp.exp(scores - peak)
         mass = jnp.sum(weights, axis=1, keepdims=True)
-        summed = dot_t(weights.astype(BF), values[512 * g : 512 * g + 512, :])
-        summed = jnp.where(diagonal, summed, 0.0)
-        summed = (summed[:, 0:128] + summed[:, 128:256]) + (summed[:, 256:384] + summed[:, 384:512])
-        sums[rows, :] = summed + pltpu.roll(summed, 64, 1)
         peaks[rows, :] = jnp.broadcast_to(peak, (32, 128))
         masses[rows, :] = jnp.broadcast_to(mass, (32, 128))
+        weights = weights.astype(BF)
+        summed = dot_t(values[512 * g : 512 * g + 512, :], jnp.concatenate([weights] * 4, axis=0))
+        total = jnp.zeros((64, 128), F32) if g % 4 == 0 else sums.pop()
+        for k in range(8):
+            own = lane // 4 == 8 * (g % 4) + k
+            total = jnp.where(own, summed[64 * k : 64 * k + 64], total)
+        sums.append(total)
 
     me = lax.axis_index("kv")
     tile = me // 2
@@ -146,67 +150,63 @@
     forget = own_scale * (forget + pltpu.roll(forget, 124, 1))
     log_forget = -(jnp.maximum(-forget, 0.0) + jnp.log1p(jnp.exp(-jnp.abs(forget))))
     log_forget = jnp.where(iota((8, 128), 1) < 4, log_forget, 0.0)
-    repeat8 = iota((32, 8), 0) // 4 == iota((32, 8), 1)
+    repeat8 = iota((128, 8), 0) // 4 % 8 == iota((128, 8), 1)
     key_value = dot(repeat8.astype(BF), key_value)
     log_forget = jnp.dot(
-        repeat8.astype(F32), log_forget, preferred_element_type=F32, precision=lax.Precision.HIGHEST
+        repeat8[0:32].astype(F32), log_forget, preferred_element_type=F32, precision=lax.Precision.HIGHEST
     )
     mine = iota((32, 128), 1) == iota((32, 128), 0) % 4
     log_forget = jnp.sum(jnp.where(mine, log_forget, 0.0), axis=1, keepdims=True)
     at = pl.ds(pl.multiple_of(32 * tile, 32), 32)
     lower = iota((32, 128), 1) < 64
-    own = jnp.sum(jnp.where(lower, query_rows[at, :] * key_value, 0.0), axis=1, keepdims=True)
+    own = jnp.sum(jnp.where(lower, query_rows[at, :] * key_value[0:32], 0.0), axis=1, keepdims=True)
     own = own * (HEAD_DIM ** (-0.5)) - log_forget
-    value = jnp.where(lower, pltpu.roll(key_value, 64, 1), key_value)
-    peak = peaks[at, :]
-    own = jnp.where(me % 2 == 0, jnp.broadcast_to(own, (32, 128)), peak - 1e30)
-    top = jnp.maximum(peak, own)
-    keep = jnp.exp(peak - top)
-    weight = jnp.exp(own - top)
-    peaks[at, :] = top
-    masses[at, :] = masses[at, :] * keep + weight
-    sums[at, :] = sums[at, :] * keep + high(weight) * value
-
-    mass = masses[...]
-    level = peaks[...] + jnp.log(mass)
-    result = sums[...] / mass
-    first = iota((128, 128), 1) < 64
-    out[0:128, :] = jnp.where(first, result[0:128], result[128:256]).astype(BF)
+    own = jnp.concatenate([own] * 4, axis=0)
     place = iota((128, 128), 0) == iota((128, 128), 1)
+    own = jnp.sum(jnp.where(place, own, 0.0), axis=0, keepdims=True)
+    pick = (iota((64, 128), 1) == iota((64, 128), 0) + 64).astype(BF)
+    value = dot_t(pick, key_value.astype(BF))
+
     line = iota((8, 128), 0)
+    slot = iota((1, 128), 1) // 32
     packed = jnp.zeros((8, 128), F32)
     for j in range(2):
-        row = jnp.sum(jnp.where(place, level[128 * j : 128 * j + 128], 0.0), axis=0, keepdims=True)
+        rows = slice(128 * j, 128 * j + 128)
+        peak = jnp.sum(jnp.where(place, peaks[rows, :], 0.0), axis=0, keepdims=True)
+        mass = jnp.sum(jnp.where(place, masses[rows, :], 0.0), axis=0, keepdims=True)
+        here = (slot + 4 * j == tile) & (me % 2 == 0)
+        joined = jnp.where(here, own, peak - 1e30)
+        top = jnp.maximum(peak, joined)
+        keep = jnp.exp(peak - top)
+        weight = jnp.exp(joined - top)
+        mass = mass * keep + weight
+        out[64 * j : 64 * j + 64, :] = ((sums[j] * keep + high(weight) * value) / mass).astype(BF)
+        level = top + jnp.log(mass)
         for k in range(3):
-            piece = high(row)
+            piece = high(level)
             packed = jnp.where(line == 3 * j + k, piece, packed)
-            row = row - piece
+            level = level - piece
     out[128:136, :] = packed.astype(BF)
 
 
 def merge_kernel(parts, w_out, out):
     extra = parts[:, 128:136, :].astype(F32)
-    factors = []
+    row, column = iota((128, 128), 0), iota((128, 128), 1)
+    order = ((row % 32 == column // 4) & (row // 32 == column % 4)).astype(BF)
+    heads = []
     for j in range(2):
         level = extra[:, 3 * j, :] + extra[:, 3 * j + 1, :] + extra[:, 3 * j + 2, :]
-        weight = jnp.exp(level - jnp.max(level, axis=0, keepdims=True))
-        factors.append(weight / jnp.sum(weight, axis=0, keepdims=True))
-    factors = jnp.concatenate(factors + [jnp.zeros((96, 128), F32)], axis=0).T
-    first = iota((128, 128), 1) < 64
-    total = jnp.zeros((128, 128), F32)
-    for i in range(16):
-        factor = jnp.where(first, factors[:, i : i + 1], factors[:, 16 + i : 17 + i])
-        total = total + parts[i, 0:128, :].astype(F32) * factor
-    turned = pltpu.roll(total, 64, 1)
-    own_lanes = iota((128, 256), 1) // HEAD_DIM == iota((128, 256), 0) % 4
-    gather = (iota((32, 128), 1) // 4 == iota((32, 128), 0)).astype(BF)
-    attended = []
-    for j in range(2):
-        half = jnp.where(first, total, turned) if j == 0 else jnp.where(first, turned, total)
-        half = jnp.where(own_lanes, jnp.concatenate([half, half], axis=1), 0.0).astype(BF)
-        attended.append(dot(gather, half))
-    attended = jnp.concatenate(attended, axis=0).astype(BF)
-    partial = dot(attended, w_out[...]).astype(BF)
+        factor = jnp.exp(level - jnp.max(level, axis=0, keepdims=True))
+        factor = factor / jnp.sum(factor, axis=0, keepdims=True)
+        total = jnp.zeros((64, 128), F32)
+        for i in range(16):
+            total = total + parts[i, 64 * j : 64 * j + 64, :].astype(F32) * factor[i : i + 1, :]
+        heads.append(dot_t(order, total.astype(BF)).astype(BF))
+    partial = jnp.zeros((64, 256), F32)
+    for h in range(4):
+        attended = jnp.concatenate([heads[0][32 * h : 32 * h + 32], heads[1][32 * h : 32 * h + 32]], axis=0)
+        partial = partial + dot(attended, w_out[64 * h : 64 * h + 64, :])
+    partial = partial.astype(BF)
     for i in range(8):
         out[i] = partial
 
@@ -291,7 +291,6 @@
             pltpu.VMEM((256, 512), BF),
             pltpu.VMEM((256, 128), F32),
             pltpu.VMEM((256, 128), F32),
-            pltpu.VMEM((256, 128), F32),
         ],
 
         limit=8 << 20,

time: 89.9 us -> 88.6 us (0.986)
  Pallas kernels: 8.55 us -> 7.22 us
    pallas_call x9, Pallas kernels: 8.55 us -> 7.22 us  [run(): pl.pallas_call(kernel, out_shape=outs, in_specs=in_specs or [VM] * len(ar...]
where the time goes in v4:
time: 88.6 us; the launch traced here: 88.3 us
  blocking collectives  79.8 us (90%)
  Pallas kernels  7.22 us (8%)
  local copies, waits for them, and re-layouts  1.06 us (1%)
    all_to_all x6, blocking collectives, exchange(): return lax.all_to_all(array, axis, split_axis=0, concat_axis=0, tiled=True)  79.8 us
    pallas_call x9, Pallas kernels, run(): pl.pallas_call(kernel, out_shape=outs, in_specs=in_specs or [VM] * len(ar...  7.22 us

profile of v4, /device:TPU:1, one launch (start us, length us, event | category | flops | bytes accessed | tf_op | source)
XLA Modules:
  0.0 88.3 jit_solution(5306703661078797485)
XLA Ops:
  0.0 0.0 slice-start
  0.1 0.0 slice-start.2
  0.1 0.7 copy-done.4
  0.8 0.0 copy-done.7
  0.8 0.0 copy-done.6
  0.8 0.2 copy-done.3
  1.0 0.2 project.1
  1.2 0.0 slice-start.1
  1.2 0.0 slice-start.3
  1.2 0.0 copy-start.11
  1.3 20.0 %all_to_all.30.parts = bf16[16,72,256]{2,1,0:T(8,128)(2,1)S(1)} all-to-all(bf16[16,72,256]{2,1,0:T(8,128)(2,1)S(1)} %spread.1), channel_id=1, replica_groups=mesh['kv'=16,'tp'=8] {'kv'}, dimensions={0} | all-to-all | bytes 1179648 | tf_op jit(solution)/shard_map/all_to_all | solution.py:267
  21.3 0.0 copy-start.2
  21.4 5.1 %attend.1 = bf16[136,128]{1,0:T(8,128)(2,1)S(1)} custom-call(bf16[16,72,256]{2,1,0:T(8,128)(2,1)S(1)} %all_to_all.30.parts, f32[1,64]{1,0:T(1,128)S(1)} %bitcast.19, bf16[4096,1024]{1,0:T(8,128)(2,1)S(1)} %bitcast.10, bf16[4096,1024]{1,0:T(8,128)(2,1)S(1)} %bitcast.13, f32[64,4,1024]{2,1,0:T(4,128)S(1)} %copy-done), custom_call_target="tpu_custom_call" | custom-call | tf_op jit(solution)/shard_map/attend/pallas_call | solution.py:49
  26.5 0.1 broadcast_in_dim.3
  26.5 13.2 %all_to_all.31.parts = bf16[16,136,128]{2,1,0:T(8,128)(2,1)S(1)} all-to-all(bf16[16,136,128]{2,1,0:T(8,128)(2,1)S(1)} %broadcast_in_dim.3), channel_id=1, replica_groups=mesh['kv'=16,'tp'=8] {'kv'}, dimensions={0} | all-to-all | bytes 1114112 | tf_op jit(solution)/shard_map/all_to_all | solution.py:267
  39.8 0.5 merge.1
  40.3 13.2 %all_to_all.32.parts = bf16[8,64,256]{2,1,0:T(8,128)(2,1)S(1)} all-to-all(bf16[8,64,256]{2,1,0:T(8,128)(2,1)S(1)} %merge.1), channel_id=1, replica_groups=mesh['kv'=16,'tp'=8] {'tp'}, dimensions={0} | all-to-all | bytes 524288 | tf_op jit(solution)/shard_map/all_to_all | solution.py:267
  53.5 0.3 up.1
  53.8 10.7 %all_to_all.33.parts = bf16[16,72,128]{2,1,0:T(8,128)(2,1)S(1)} all-to-all(bf16[16,72,128]{2,1,0:T(8,128)(2,1)S(1)} %get-tuple-element.11), channel_id=1, replica_groups=mesh['kv'=16,'tp'=8] {'kv'}, dimensions={0} | all-to-all | bytes 589824 | tf_op jit(solution)/shard_map/all_to_all | solution.py:267
  64.5 0.1 hidden.1
  64.6 10.2 %all_to_all.34.parts = bf16[16,64,128]{2,1,0:T(8,128)(2,1)S(1)} all-to-all(bf16[16,64,128]{2,1,0:T(8,128)(2,1)S(1)} %hidden.1), channel_id=1, replica_groups=mesh['kv'=16,'tp'=8] {'kv'}, dimensions={0} | all-to-all | bytes 524288 | tf_op jit(solution)/shard_map/all_to_all | solution.py:267
  74.9 0.3 down.1
  75.2 12.5 %all_to_all.35.parts = bf16[8,64,256]{2,1,0:T(8,128)(2,1)S(1)} all-to-all(bf16[8,64,256]{2,1,0:T(8,128)(2,1)S(1)} %down.1), channel_id=1, replica_groups=mesh['kv'=16,'tp'=8] {'tp'}, dimensions={0} | all-to-all | bytes 524288 | tf_op jit(solution)/shard_map/all_to_all | solution.py:267
  87.7 0.7 finish.1
  (26 shorter events, 0.1 us)
Async XLA Ops:
  0.0 0.8 copy-start.4
  0.0 0.8 copy-start.8
  0.0 0.8 copy-start.7
  0.0 0.8 copy-start.6
  0.0 1.0 %copy-start.3 = (bf16[256,256]{1,0:T(8,128)(2,1)S(1)}, bf16[256,256]{1,0:T(8,128)(2,1)}, u32[]{:S(2)}) copy-start(bf16[256,256]{1,0:T(8,128)(2,1)} %w_query.1) | copy-start | bytes 393220
  0.0 1.0 %copy-start.10 = (f32[256]{0:T(256)S(1)}, f32[256]{0:T(256)}, u32[]{:S(2)}) copy-start(f32[256]{0:T(256)} %param.15) | copy-start | bytes 3076
  0.0 21.2 %slice-start = ((s8[8388608]{0:T(1024)(128)(4,1)}), s8[4194304]{0:T(1024)(128)(4,1)S(1)}, s32[]{:S(2)}) async-start(s8[8388608]{0:T(1024)(128)(4,1)} %bitcast.8), calls=%async_computation.6 | async-start | bytes 8388608
  0.1 21.2 %slice-start.2 = ((s8[8388608]{0:T(1024)(128)(4,1)}), s8[4194304]{0:T(1024)(128)(4,1)S(1)}, s32[]{:S(2)}) async-start(s8[8388608]{0:T(1024)(128)(4,1)} %bitcast.11), calls=%async_computation.8 | async-start | bytes 8388608
  1.2 20.1 %slice-start.1 = ((s8[8388608]{0:T(1024)(128)(4,1)}), s8[4194304]{0:T(1024)(128)(4,1)S(1)}, s32[]{:S(2)}) async-start(s8[8388608]{0:T(1024)(128)(4,1)} %bitcast.8), calls=%async_computation.7 | async-start | bytes 8388608
  1.2 20.1 %slice-start.3 = ((s8[8388608]{0:T(1024)(128)(4,1)}), s8[4194304]{0:T(1024)(128)(4,1)S(1)}, s32[]{:S(2)}) async-start(s8[8388608]{0:T(1024)(128)(4,1)} %bitcast.11), calls=%async_computation.9 | async-start | bytes 8388608
  1.2 20.1 %copy-start = (f32[64,4,1024]{2,1,0:T(4,128)S(1)}, f32[64,4,1024]{2,1,0:T(4,128)}, u32[]{:S(2)}) copy-start(f32[64,4,1024]{2,1,0:T(4,128)} %decay.1) | copy-start | bytes 3145732
  1.2 20.1 %copy-start.11 = (f32[64]{0:T(128)S(1)}, f32[64]{0:T(128)}, u32[]{:S(2)}) copy-start(f32[64]{0:T(128)} %param.20) | copy-start | bytes 772
  21.3 18.5 %copy-start.5 = (bf16[256,256]{1,0:T(8,128)(2,1)S(1)}, bf16[256,256]{1,0:T(8,128)(2,1)}, u32[]{:S(2)}) copy-start(bf16[256,256]{1,0:T(8,128)(2,1)} %w_out.1) | copy-start | bytes 393220
  21.3 32.2 %copy-start.2 = (bf16[256,2048]{1,0:T(8,128)(2,1)S(1)}, bf16[256,2048]{1,0:T(8,128)(2,1)}, u32[]{:S(2)}) copy-start(bf16[256,2048]{1,0:T(8,128)(2,1)} %w_up.1) | copy-start | bytes 3145732
  21.3 32.2 %copy-start.9 = (f32[256]{0:T(256)S(1)}, f32[256]{0:T(256)}, u32[]{:S(2)}) copy-start(f32[256]{0:T(256)} %param.25) | copy-start | bytes 3076
  21.3 53.5 %copy-start.1 = (bf16[2048,256]{1,0:T(8,128)(2,1)S(1)}, bf16[2048,256]{1,0:T(8,128)(2,1)}, u32[]{:S(2)}) copy-start(bf16[2048,256]{1,0:T(8,128)(2,1)} %w_down.1) | copy-start | bytes 3145732

commit v5 on v4

--- a/solution.py
+++ b/solution.py
@@ -1,5 +1,3 @@
-import functools
-
 import jax
 import jax.numpy as jnp
 from jax import lax
@@ -93,24 +91,24 @@
     parts, query_gain, keys, values, decay, out,
     scales, query_rows, left, peaks, masses,
 ):
-    raw = parts[0, 0:64, :].astype(F32)
-    extra = parts[0, 64:72, :].astype(F32)
-    for i in range(1, 16):
-        raw = raw + parts[i, 0:64, :].astype(F32)
-        extra = extra + parts[i, 64:72, :].astype(F32)
+    extra = [parts[i, 64:72, :].astype(F32) for i in range(16)]
+    raw = [parts[i, 0:64, :].astype(F32) for i in range(16)]
+    while len(raw) > 1:
+        raw = [a + b for a, b in zip(raw[::2], raw[1::2])]
+        extra = [a + b for a, b in zip(extra[::2], extra[1::2])]
+    raw, extra = raw[0], extra[0]
     squares = row_to_column(extra[0:1, 128:256] + extra[1:2, 128:256], 64, 64)
     scale = lax.rsqrt(squares / D + EPS)
     scales[...] = jnp.broadcast_to(scale, (64, 128))
-    heads = scale * raw
     head_of = iota((64, 256), 1) // HEAD_DIM
-    power = heads * heads
+    power = raw * raw
     inverse = jnp.zeros((64, 256), F32)
     for h in range(4):
         mean = jnp.sum(jnp.where(head_of == h, power, 0.0), axis=1, keepdims=True) / HEAD_DIM
-        inverse = jnp.where(head_of == h, lax.rsqrt(mean + EPS), inverse)
+        inverse = jnp.where(head_of == h, scale * lax.rsqrt(scale * scale * mean + EPS), inverse)
     gain = query_gain[...]
     gain = jnp.concatenate([gain, gain, gain, gain], axis=1)
-    query = (heads * inverse * gain).astype(BF)
+    query = (raw * inverse * gain).astype(BF)
 
     repeat = (iota((256, 64), 0) // 4 == iota((256, 64), 1)).astype(BF)
     spread = dot(repeat, query)
@@ -119,28 +117,9 @@
     folded = spread[:, 0:128] + spread[:, 128:256]
     folded = folded + pltpu.roll(folded, 64, 1)
     query_rows[...] = folded
-    wide = jnp.concatenate([folded] * 4, axis=1)
-    block = iota((256, 512), 1) // HEAD_DIM == (iota((256, 512), 0) // 4) % 8
-    left[...] = jnp.where(block, wide, 0.0).astype(BF)
-
-    lane = iota((64, 128), 1)
-    sums = []
-    for g in range(8):
-        rows = slice(32 * g, 32 * g + 32)
-        scores = dot(left[rows, :], keys[512 * g : 512 * g + 512, :]) * (HEAD_DIM ** (-0.5))
-        scores = scores + decay[8 * g : 8 * g + 8].reshape(32, 1024)
-        peak = jnp.max(scores, axis=1, keepdims=True)
-        weights = jnp.exp(scores - peak)
-        mass = jnp.sum(weights, axis=1, keepdims=True)
-        peaks[rows, :] = jnp.broadcast_to(peak, (32, 128))
-        masses[rows, :] = jnp.broadcast_to(mass, (32, 128))
-        weights = weights.astype(BF)
-        summed = dot_t(values[512 * g : 512 * g + 512, :], jnp.concatenate([weights] * 4, axis=0))
-        total = jnp.zeros((64, 128), F32) if g % 4 == 0 else sums.pop()
-        for k in range(8):
-            own = lane // 4 == 8 * (g % 4) + k
-            total = jnp.where(own, summed[64 * k : 64 * k + 64], total)
-        sums.append(total)
+    wide = jnp.concatenate([folded] * 2, axis=1)
+    block = iota((256, 256), 1) // HEAD_DIM == (iota((256, 256), 0) // 4) % 4
+    left[...] = jnp.where(block, wide * (HEAD_DIM ** (-0.5)), 0.0).astype(BF)
 
     me = lax.axis_index("kv")
     tile = me // 2
@@ -167,6 +146,31 @@
     pick = (iota((64, 128), 1) == iota((64, 128), 0) + 64).astype(BF)
     value = dot_t(pick, key_value.astype(BF))
 
+    lane = iota((64, 16), 1)
+    folds = []
+    def score(g):
+        scores = dot(left[16 * g : 16 * g + 16, :], keys[256 * g : 256 * g + 256, :])
+        return scores + decay[4 * g : 4 * g + 4].reshape(16, 1024)
+
+    ahead = [score(g) for g in range(8)]
+    for g in range(16):
+        rows = slice(16 * g, 16 * g + 16)
+        scores = ahead.pop(0)
+        peak = jnp.max(scores, axis=1, keepdims=True)
+        weights = jnp.exp(scores - peak)
+        mass = jnp.sum(weights, axis=1, keepdims=True)
+        peaks[rows, :] = jnp.broadcast_to(peak, (16, 128))
+        masses[rows, :] = jnp.broadcast_to(mass, (16, 128))
+        weights = weights.astype(BF)
+        if g + 8 < 16:
+            ahead.append(score(g + 8))
+        summed = dot_t(values[256 * g : 256 * g + 256, :], weights)
+        total = summed[0:64]
+        for k in range(1, 4):
+            total = jnp.where(lane // 4 == k, summed[64 * k : 64 * k + 64], total)
+        folds.append(total)
+    sums = [jnp.concatenate(folds[8 * j : 8 * j + 8], axis=1) for j in range(2)]
+
     line = iota((8, 128), 0)
     slot = iota((1, 128), 1) // 32
     packed = jnp.zeros((8, 128), F32)
@@ -271,6 +275,28 @@
     return exchange(jnp.broadcast_to(array, (lax.axis_size(axis), *array.shape)), axis)
 
 
+def attend(message, query_gain, key_cache, value_cache, decay_cache):
+    return call(
+        attend_kernel,
+        jax.ShapeDtypeStruct((136, 128), BF),
+        "attend",
+        scratch=[
+            pltpu.VMEM((64, 128), F32),
+            pltpu.VMEM((256, 128), F32),
+            pltpu.VMEM((256, 256), BF),
+            pltpu.VMEM((256, 128), F32),
+            pltpu.VMEM((256, 128), F32),
+        ],
+        limit=8 << 20,
+    )(
+        message,
+        query_gain.reshape(1, -1),
+        key_cache.reshape(4096, 1024),
+        value_cache.reshape(4096, 1024),
+        decay_cache,
+    )
+
+
 def shards(
     tokens, mix_gain, w_query, w_key, w_value, w_forget, query_gain,
     key_cache, value_cache, decay_cache, w_out, mlp_gain, w_up, w_down,
@@ -281,26 +307,7 @@
     query, extra = call(project_kernel, (shape((64, 256), BF), shape((64, 256), BF)), "project")(head, *operands)
     message = call(spread_kernel, shape((16, 72, 256), BF), "spread", cost=10**10)(query, extra)
     message = exchange(message, "kv")
-    part = call(
-        attend_kernel,
-        shape((136, 128), BF),
-        "attend",
-        scratch=[
-            pltpu.VMEM((64, 128), F32),
-            pltpu.VMEM((256, 128), F32),
-            pltpu.VMEM((256, 512), BF),
-            pltpu.VMEM((256, 128), F32),
-            pltpu.VMEM((256, 128), F32),
-        ],
-
-        limit=8 << 20,
-    )(
-        message,
-        query_gain.reshape(1, -1),
-        key_cache.reshape(4096, 1024),
-        value_cache.reshape(4096, 1024),
-        decay_cache,
-    )
+    part = attend(message, query_gain, key_cache, value_cache, decay_cache)
     message = call(merge_kernel, shape((8, 64, 256), BF), "merge")(sent(part, "kv"), w_out)
     residual, message = call(up_kernel, (shape((64, 256), BF), shape((16, 72, 128), BF)), "up")(
         exchange(message, "tp"), tokens, mlp_gain.reshape(1, -1), w_up

time: 88.6 us -> 87.3 us (0.985)
  Pallas kernels: 7.22 us -> 5.92 us
    pallas_call x9, Pallas kernels: 7.22 us -> 5.92 us  [run(): pl.pallas_call(kernel, out_shape=outs, in_specs=in_specs or [VM] * len(ar...]
where the time goes in v5:
time: 87.3 us; the launch traced here: 87 us
  blocking collectives  79.8 us (91%)
  Pallas kernels  5.92 us (7%)
  local copies, waits for them, and re-layouts  1.06 us (1%)
    all_to_all x6, blocking collectives, exchange(): return lax.all_to_all(array, axis, split_axis=0, concat_axis=0, tiled=True)  79.8 us
    pallas_call x9, Pallas kernels, run(): pl.pallas_call(kernel, out_shape=outs, in_specs=in_specs or [VM] * len(ar...  5.92 us

profile of v5, /device:TPU:1, one launch (start us, length us, event | category | flops | bytes accessed | tf_op | source)
XLA Modules:
  0.0 87.0 jit_solution(18308940744410926348)
XLA Ops:
  0.0 0.0 slice-start
  0.1 0.0 slice-start.2
  0.1 0.7 copy-done.4
  0.8 0.0 copy-done.7
  0.8 0.0 copy-done.6
  0.8 0.2 copy-done.3
  1.0 0.2 project.1
  1.2 0.0 slice-start.1
  1.2 0.0 slice-start.3
  1.2 0.0 copy-start.11
  1.3 20.0 %all_to_all.30.parts = bf16[16,72,256]{2,1,0:T(8,128)(2,1)S(1)} all-to-all(bf16[16,72,256]{2,1,0:T(8,128)(2,1)S(1)} %spread.1), channel_id=1, replica_groups=mesh['kv'=16,'tp'=8] {'kv'}, dimensions={0} | all-to-all | bytes 1179648 | tf_op jit(solution)/shard_map/all_to_all | solution.py:271
  21.3 0.0 copy-start.2
  21.4 3.8 %attend.1 = bf16[136,128]{1,0:T(8,128)(2,1)S(1)} custom-call(bf16[16,72,256]{2,1,0:T(8,128)(2,1)S(1)} %all_to_all.30.parts, f32[1,64]{1,0:T(1,128)S(1)} %bitcast.19, bf16[4096,1024]{1,0:T(8,128)(2,1)S(1)} %bitcast.10, bf16[4096,1024]{1,0:T(8,128)(2,1)S(1)} %bitcast.13, f32[64,4,1024]{2,1,0:T(4,128)S(1)} %copy-done), custom_call_target="tpu_custom_call" | custom-call | tf_op jit(solution)/shard_map/attend/pallas_call | solution.py:47
  25.2 0.1 broadcast_in_dim.3
  25.3 13.2 %all_to_all.31.parts = bf16[16,136,128]{2,1,0:T(8,128)(2,1)S(1)} all-to-all(bf16[16,136,128]{2,1,0:T(8,128)(2,1)S(1)} %broadcast_in_dim.3), channel_id=1, replica_groups=mesh['kv'=16,'tp'=8] {'kv'}, dimensions={0} | all-to-all | bytes 1114112 | tf_op jit(solution)/shard_map/all_to_all | solution.py:271
  38.5 0.5 merge.1
  38.9 13.2 %all_to_all.32.parts = bf16[8,64,256]{2,1,0:T(8,128)(2,1)S(1)} all-to-all(bf16[8,64,256]{2,1,0:T(8,128)(2,1)S(1)} %merge.1), channel_id=1, replica_groups=mesh['kv'=16,'tp'=8] {'tp'}, dimensions={0} | all-to-all | bytes 524288 | tf_op jit(solution)/shard_map/all_to_all | solution.py:271
  52.2 0.3 up.1
  52.5 10.7 %all_to_all.33.parts = bf16[16,72,128]{2,1,0:T(8,128)(2,1)S(1)} all-to-all(bf16[16,72,128]{2,1,0:T(8,128)(2,1)S(1)} %get-tuple-element.11), channel_id=1, replica_groups=mesh['kv'=16,'tp'=8] {'kv'}, dimensions={0} | all-to-all | bytes 589824 | tf_op jit(solution)/shard_map/all_to_all | solution.py:271
  63.2 0.1 hidden.1
  63.3 10.2 %all_to_all.34.parts = bf16[16,64,128]{2,1,0:T(8,128)(2,1)S(1)} all-to-all(bf16[16,64,128]{2,1,0:T(8,128)(2,1)S(1)} %hidden.1), channel_id=1, replica_groups=mesh['kv'=16,'tp'=8] {'kv'}, dimensions={0} | all-to-all | bytes 524288 | tf_op jit(solution)/shard_map/all_to_all | solution.py:271
  73.6 0.3 down.1
  73.9 12.5 %all_to_all.35.parts = bf16[8,64,256]{2,1,0:T(8,128)(2,1)S(1)} all-to-all(bf16[8,64,256]{2,1,0:T(8,128)(2,1)S(1)} %down.1), channel_id=1, replica_groups=mesh['kv'=16,'tp'=8] {'tp'}, dimensions={0} | all-to-all | bytes 524288 | tf_op jit(solution)/shard_map/all_to_all | solution.py:271
  86.4 0.7 finish.1
  (26 shorter events, 0.1 us)
Async XLA Ops:
  0.0 0.8 copy-start.4
  0.0 0.8 copy-start.8
  0.0 0.8 copy-start.7
  0.0 0.8 copy-start.6
  0.0 1.0 %copy-start.3 = (bf16[256,256]{1,0:T(8,128)(2,1)S(1)}, bf16[256,256]{1,0:T(8,128)(2,1)}, u32[]{:S(2)}) copy-start(bf16[256,256]{1,0:T(8,128)(2,1)} %w_query.1) | copy-start | bytes 393220
  0.0 1.0 %copy-start.10 = (f32[256]{0:T(256)S(1)}, f32[256]{0:T(256)}, u32[]{:S(2)}) copy-start(f32[256]{0:T(256)} %param.15) | copy-start | bytes 3076
  0.0 21.2 %slice-start = ((s8[8388608]{0:T(1024)(128)(4,1)}), s8[4194304]{0:T(1024)(128)(4,1)S(1)}, s32[]{:S(2)}) async-start(s8[8388608]{0:T(1024)(128)(4,1)} %bitcast.8), calls=%async_computation.6 | async-start | bytes 8388608
  0.1 21.2 %slice-start.2 = ((s8[8388608]{0:T(1024)(128)(4,1)}), s8[4194304]{0:T(1024)(128)(4,1)S(1)}, s32[]{:S(2)}) async-start(s8[8388608]{0:T(1024)(128)(4,1)} %bitcast.11), calls=%async_computation.8 | async-start | bytes 8388608
  1.2 20.1 %slice-start.1 = ((s8[8388608]{0:T(1024)(128)(4,1)}), s8[4194304]{0:T(1024)(128)(4,1)S(1)}, s32[]{:S(2)}) async-start(s8[8388608]{0:T(1024)(128)(4,1)} %bitcast.8), calls=%async_computation.7 | async-start | bytes 8388608
  1.2 20.1 %slice-start.3 = ((s8[8388608]{0:T(1024)(128)(4,1)}), s8[4194304]{0:T(1024)(128)(4,1)S(1)}, s32[]{:S(2)}) async-start(s8[8388608]{0:T(1024)(128)(4,1)} %bitcast.11), calls=%async_computation.9 | async-start | bytes 8388608
  1.2 20.1 %copy-start = (f32[64,4,1024]{2,1,0:T(4,128)S(1)}, f32[64,4,1024]{2,1,0:T(4,128)}, u32[]{:S(2)}) copy-start(f32[64,4,1024]{2,1,0:T(4,128)} %decay.1) | copy-start | bytes 3145732
  1.2 20.1 %copy-start.11 = (f32[64]{0:T(128)S(1)}, f32[64]{0:T(128)}, u32[]{:S(2)}) copy-start(f32[64]{0:T(128)} %param.20) | copy-start | bytes 772
  21.3 17.1 %copy-start.5 = (bf16[256,256]{1,0:T(8,128)(2,1)S(1)}, bf16[256,256]{1,0:T(8,128)(2,1)}, u32[]{:S(2)}) copy-start(bf16[256,256]{1,0:T(8,128)(2,1)} %w_out.1) | copy-start | bytes 393220
  21.3 30.9 %copy-start.2 = (bf16[256,2048]{1,0:T(8,128)(2,1)S(1)}, bf16[256,2048]{1,0:T(8,128)(2,1)}, u32[]{:S(2)}) copy-start(bf16[256,2048]{1,0:T(8,128)(2,1)} %w_up.1) | copy-start | bytes 3145732
  21.3 30.9 %copy-start.9 = (f32[256]{0:T(256)S(1)}, f32[256]{0:T(256)}, u32[]{:S(2)}) copy-start(f32[256]{0:T(256)} %param.25) | copy-start | bytes 3076
  21.3 52.2 %copy-start.1 = (bf16[2048,256]{1,0:T(8,128)(2,1)S(1)}, bf16[2048,256]{1,0:T(8,128)(2,1)}, u32[]{:S(2)}) copy-start(bf16[2048,256]{1,0:T(8,128)(2,1)} %w_down.1) | copy-start | bytes 3145732

commit v6 on v5

--- a/solution.py
+++ b/solution.py
@@ -3,11 +3,13 @@
 from jax import lax
 from jax.experimental import pallas as pl
 from jax.experimental.pallas import tpu as pltpu
+from jax.sharding import Mesh
 from jax.sharding import PartitionSpec as P
 
 D = 4096
 HEAD_DIM = 64
 EPS = 1e-06
+TP = ("x", "core")
 BF = jnp.bfloat16
 F32 = jnp.float32
 
@@ -210,14 +212,18 @@
     for h in range(4):
         attended = jnp.concatenate([heads[0][32 * h : 32 * h + 32], heads[1][32 * h : 32 * h + 32]], axis=0)
         partial = partial + dot(attended, w_out[64 * h : 64 * h + 64, :])
-    partial = partial.astype(BF)
-    for i in range(8):
-        out[i] = partial
+    out[...] = partial.astype(BF)
+
+
+def pair_kernel(mine, partner, out):
+    total = (mine[...].astype(F32) + partner[...].astype(F32)).astype(BF)
+    for i in range(4):
+        out[i] = total
 
 
 def up_kernel(parts, tokens, gain, w_up, residual_out, out):
     attn = parts[0].astype(F32)
-    for i in range(1, 8):
+    for i in range(1, 4):
         attn = attn + parts[i].astype(F32)
     residual = (tokens[...].astype(F32) + high(attn)).astype(BF)
     residual_out[...] = residual
@@ -255,20 +261,24 @@
     for i in range(0, 16, 2):
         pair = jnp.concatenate([parts[i], parts[i + 1]], axis=1)
         down = down + dot(pair, w_down[128 * i : 128 * i + 256, :])
-    down = down.astype(BF)
-    for i in range(8):
-        out[i] = down
+    out[...] = down.astype(BF)
 
 
 def finish_kernel(parts, residual, out):
     down = parts[0].astype(F32)
-    for i in range(1, 8):
+    for i in range(1, 4):
         down = down + parts[i].astype(F32)
     out[...] = (residual[...].astype(F32) + high(down)).astype(BF)
 
 
 def exchange(array, axis):
     return lax.all_to_all(array, axis, split_axis=0, concat_axis=0, tiled=True)
+
+
+def pair_sum(partial):
+    partner = lax.ppermute(partial, "core", [(0, 1), (1, 0)])
+    message = call(pair_kernel, jax.ShapeDtypeStruct((4, 64, 256), BF), "pair")(partial, partner)
+    return exchange(message, "x")
 
 
 def sent(array, axis):
@@ -308,34 +318,35 @@
     message = call(spread_kernel, shape((16, 72, 256), BF), "spread", cost=10**10)(query, extra)
     message = exchange(message, "kv")
     part = attend(message, query_gain, key_cache, value_cache, decay_cache)
-    message = call(merge_kernel, shape((8, 64, 256), BF), "merge")(sent(part, "kv"), w_out)
+    partial = call(merge_kernel, shape((64, 256), BF), "merge")(sent(part, "kv"), w_out)
     residual, message = call(up_kernel, (shape((64, 256), BF), shape((16, 72, 128), BF)), "up")(
-        exchange(message, "tp"), tokens, mlp_gain.reshape(1, -1), w_up
+        pair_sum(partial), tokens, mlp_gain.reshape(1, -1), w_up
     )
     message = call(hidden_kernel, shape((16, 64, 128), BF), "hidden")(exchange(message, "kv"))
-    message = call(down_kernel, shape((8, 64, 256), BF), "down")(exchange(message, "kv"), w_down)
-    return call(finish_kernel, shape((64, 256), BF), "finish")(exchange(message, "tp"), residual)
+    partial = call(down_kernel, shape((64, 256), BF), "down")(exchange(message, "kv"), w_down)
+    return call(finish_kernel, shape((64, 256), BF), "finish")(pair_sum(partial), residual)
 
 
 def solution(mesh):
+    split = Mesh(mesh.devices.reshape(mesh.shape["kv"], -1, 2), ("kv", "x", "core"))
     return jax.shard_map(
         shards,
-        mesh=mesh,
+        mesh=split,
         in_specs=(
             P(None, "kv"),
             P("kv"),
-            P("kv", "tp"),
-            P("kv", "tp"),
-            P("kv", "tp"),
-            P("kv", "tp"),
+            P("kv", TP),
+            P("kv", TP),
+            P("kv", TP),
+            P("kv", TP),
             P(),
-            P(None, "tp", None, "kv"),
-            P(None, "tp", None, "kv"),
-            P(None, "tp", "kv"),
-            P("tp", "kv"),
+            P(None, TP, None, "kv"),
+            P(None, TP, None, "kv"),
+            P(None, TP, "kv"),
+            P(TP, "kv"),
             P("kv"),
-            P("kv", "tp"),
-            P("tp", "kv"),
+            P("kv", TP),
+            P(TP, "kv"),
         ),
         out_specs=P(None, "kv"),
         check_vma=False,

time: 87.3 us -> 86.5 us (level)
  blocking collectives: 79.8 us -> 70 us
  starting transfers between devices: 0 us -> 7.16 us
  waiting for transfers between devices: 0 us -> 1.72 us
    all_to_all x6, blocking collectives: 79.8 us -> 70 us  [exchange(): return lax.all_to_all(array, axis, split_axis=0, concat_axis=0, tiled=True)]
    ppermute x0 -> x2, starting transfers between devices: none -> 7.16 us  [pair_sum(): partner = lax.ppermute(partial, 'core', [(0, 1), (1, 0)])]
    ppermute x0 -> x2, waiting for transfers between devices: none -> 1.72 us  [pair_sum(): partner = lax.ppermute(partial, 'core', [(0, 1), (1, 0)])]
    pallas_call x9 -> x11, Pallas kernels: 5.92 us -> 5.9 us  [run(): pl.pallas_call(kernel, out_shape=outs, in_specs=in_specs or [VM] * len(ar...]
  transfers between devices with their start and end apart: 0 -> 2, of which waited for: 0 -> 2; matrix products, arithmetic and copies ran while one was open for 0% -> 0% of each run, Pallas kernels for 0% -> 0%
where the time goes in v6:
time: 86.5 us; the launch traced here: 86.1 us
  blocking collectives  70 us (81%)
  starting transfers between devices  7.16 us (8%)
  Pallas kernels  5.9 us (7%)
  waiting for transfers between devices  1.72 us (2%)
  local copies, waits for them, and re-layouts  1.06 us (1%)
    all_to_all x6, blocking collectives, exchange(): return lax.all_to_all(array, axis, split_axis=0, concat_axis=0, tiled=True)  70 us
    ppermute x2, starting transfers between devices, pair_sum(): partner = lax.ppermute(partial, 'core', [(0, 1), (1, 0)])  7.16 us
    pallas_call x11, Pallas kernels, run(): pl.pallas_call(kernel, out_shape=outs, in_specs=in_specs or [VM] * len(ar...  5.9 us
  transfers between devices with their start and end apart: 2, of which 2 were waited for; matrix products, arithmetic and copies ran while one was open for 0% of the time, Pallas kernels for 0%

profile of v6, /device:TPU:1, one launch (start us, length us, event | category | flops | bytes accessed | tf_op | source)
XLA Modules:
  0.0 86.1 jit_solution(18013168550091008095)
XLA Ops:
  0.1 0.7 copy-done.5
  0.8 0.0 copy-done.7
  0.8 0.0 copy-done.6
  0.8 0.2 copy-done.3
  1.0 0.2 project.1
  1.2 0.0 slice-start.1
  1.2 0.0 slice-start.3
  1.3 20.0 %all_to_all.30.parts = bf16[16,72,256]{2,1,0:T(8,128)(2,1)S(1)} all-to-all(bf16[16,72,256]{2,1,0:T(8,128)(2,1)S(1)} %spread.1), channel_id=1, replica_groups=mesh['kv'=16,'x'=4,'core'=2] {'kv'}, dimensions={0} | all-to-all | bytes 1179648 | tf_op jit(solution)/shard_map/all_to_all | solution.py:275
  21.4 3.8 %attend.1 = bf16[136,128]{1,0:T(8,128)(2,1)S(1)} custom-call(bf16[16,72,256]{2,1,0:T(8,128)(2,1)S(1)} %all_to_all.30.parts, f32[1,64]{1,0:T(1,128)S(1)} %bitcast.19, bf16[4096,1024]{1,0:T(8,128)(2,1)S(1)} %bitcast.10, bf16[4096,1024]{1,0:T(8,128)(2,1)S(1)} %bitcast.13, f32[64,4,1024]{2,1,0:T(4,128)S(1)} %copy-done), custom_call_target="tpu_custom_call" | custom-call | tf_op jit(solution)/shard_map/attend/pallas_call | solution.py:49
  25.2 0.1 broadcast_in_dim.3
  25.3 13.2 %all_to_all.31.parts = bf16[16,136,128]{2,1,0:T(8,128)(2,1)S(1)} all-to-all(bf16[16,136,128]{2,1,0:T(8,128)(2,1)S(1)} %broadcast_in_dim.3), channel_id=1, replica_groups=mesh['kv'=16,'x'=4,'core'=2] {'kv'}, dimensions={0} | all-to-all | bytes 1114112 | tf_op jit(solution)/shard_map/all_to_all | solution.py:275
  38.5 0.5 merge.1.mine
  38.9 2.8 %collective-permute-start = (bf16[64,256]{1,0:T(8,128)(2,1)S(1)}, bf16[64,256]{1,0:T(8,128)(2,1)S(1)}, u32[]{:S(2)}, u32[]{:S(2)}) collective-permute-start(bf16[64,256]{1,0:T(8,128)(2,1)S(1)} %merge.1.mine), channel_id=1, source_target_pairs={{0,1},{1,0},{2,3},{3,2},{4,5},{5,4},{6,7},{7,6},{8,9},{9,8},{10,11... | collective-permute-start | bytes 98312 | tf_op jit(solution)/shard_map/ppermute | solution.py:279
  41.7 0.9 collective-permute-done.partner
  42.6 8.6 %all_to_all.32.parts = bf16[4,64,256]{2,1,0:T(8,128)(2,1)S(1)} all-to-all(bf16[4,64,256]{2,1,0:T(8,128)(2,1)S(1)} %pair.2), channel_id=1, replica_groups=mesh['kv'=16,'x'=4,'core'=2] {'x'}, dimensions={0} | all-to-all | bytes 262144 | tf_op jit(solution)/shard_map/all_to_all | solution.py:275
  51.2 0.3 up.1
  51.5 10.5 %all_to_all.33.parts = bf16[16,72,128]{2,1,0:T(8,128)(2,1)S(1)} all-to-all(bf16[16,72,128]{2,1,0:T(8,128)(2,1)S(1)} %get-tuple-element.11), channel_id=1, replica_groups=mesh['kv'=16,'x'=4,'core'=2] {'kv'}, dimensions={0} | all-to-all | bytes 589824 | tf_op jit(solution)/shard_map/all_to_all | solution.py:275
  62.0 0.1 hidden.1
  62.2 10.4 %all_to_all.34.parts = bf16[16,64,128]{2,1,0:T(8,128)(2,1)S(1)} all-to-all(bf16[16,64,128]{2,1,0:T(8,128)(2,1)S(1)} %hidden.1), channel_id=1, replica_groups=mesh['kv'=16,'x'=4,'core'=2] {'kv'}, dimensions={0} | all-to-all | bytes 524288 | tf_op jit(solution)/shard_map/all_to_all | solution.py:275
  72.6 0.3 down.1.mine
  72.9 4.4 %collective-permute-start.1 = (bf16[64,256]{1,0:T(8,128)(2,1)S(1)}, bf16[64,256]{1,0:T(8,128)(2,1)S(1)}, u32[]{:S(2)}, u32[]{:S(2)}) collective-permute-start(bf16[64,256]{1,0:T(8,128)(2,1)S(1)} %down.1.mine), channel_id=1, source_target_pairs={{0,1},{1,0},{2,3},{3,2},{4,5},{5,4},{6,7},{7,6},{8,9},{9,8},{10,11... | collective-permute-start | bytes 98312 | tf_op jit(solution)/shard_map/ppermute | solution.py:279
  77.3 0.9 collective-permute-done.1.partner
  78.2 7.2 %all_to_all.35.parts = bf16[4,64,256]{2,1,0:T(8,128)(2,1)S(1)} all-to-all(bf16[4,64,256]{2,1,0:T(8,128)(2,1)S(1)} %pair.3), channel_id=1, replica_groups=mesh['kv'=16,'x'=4,'core'=2] {'x'}, dimensions={0} | all-to-all | bytes 262144 | tf_op jit(solution)/shard_map/all_to_all | solution.py:275
  85.4 0.6 finish.1
  (32 shorter events, 0.1 us)
Async XLA Ops:
  0.0 0.8 copy-start.5
  0.0 0.8 copy-start.8
  0.0 0.8 copy-start.7
  0.0 0.8 copy-start.6
  0.0 1.0 %copy-start.3 = (bf16[256,256]{1,0:T(8,128)(2,1)S(1)}, bf16[256,256]{1,0:T(8,128)(2,1)}, u32[]{:S(2)}) copy-start(bf16[256,256]{1,0:T(8,128)(2,1)} %w_query.1) | copy-start | bytes 393220
  0.0 1.0 %copy-start.9 = (f32[256]{0:T(256)S(1)}, f32[256]{0:T(256)}, u32[]{:S(2)}) copy-start(f32[256]{0:T(256)} %param.15) | copy-start | bytes 3076
  0.0 21.2 %slice-start = ((s8[8388608]{0:T(1024)(128)(4,1)}), s8[4194304]{0:T(1024)(128)(4,1)S(1)}, s32[]{:S(2)}) async-start(s8[8388608]{0:T(1024)(128)(4,1)} %bitcast.8), calls=%async_computation.6 | async-start | bytes 8388608
  0.1 21.2 %slice-start.2 = ((s8[8388608]{0:T(1024)(128)(4,1)}), s8[4194304]{0:T(1024)(128)(4,1)S(1)}, s32[]{:S(2)}) async-start(s8[8388608]{0:T(1024)(128)(4,1)} %bitcast.11), calls=%async_computation.8 | async-start | bytes 8388608
  1.2 20.1 %slice-start.1 = ((s8[8388608]{0:T(1024)(128)(4,1)}), s8[4194304]{0:T(1024)(128)(4,1)S(1)}, s32[]{:S(2)}) async-start(s8[8388608]{0:T(1024)(128)(4,1)} %bitcast.8), calls=%async_computation.7 | async-start | bytes 8388608
  1.2 20.1 %slice-start.3 = ((s8[8388608]{0:T(1024)(128)(4,1)}), s8[4194304]{0:T(1024)(128)(4,1)S(1)}, s32[]{:S(2)}) async-start(s8[8388608]{0:T(1024)(128)(4,1)} %bitcast.11), calls=%async_computation.9 | async-start | bytes 8388608
  1.2 20.1 %copy-start = (f32[64,4,1024]{2,1,0:T(4,128)S(1)}, f32[64,4,1024]{2,1,0:T(4,128)}, u32[]{:S(2)}) copy-start(f32[64,4,1024]{2,1,0:T(4,128)} %decay.1) | copy-start | bytes 3145732
  1.2 20.1 %copy-start.11 = (f32[64]{0:T(128)S(1)}, f32[64]{0:T(128)}, u32[]{:S(2)}) copy-start(f32[64]{0:T(128)} %param.20) | copy-start | bytes 772
  21.3 17.1 %copy-start.4 = (bf16[256,256]{1,0:T(8,128)(2,1)S(1)}, bf16[256,256]{1,0:T(8,128)(2,1)}, u32[]{:S(2)}) copy-start(bf16[256,256]{1,0:T(8,128)(2,1)} %w_out.1) | copy-start | bytes 393220
  21.3 29.9 %copy-start.1 = (bf16[256,2048]{1,0:T(8,128)(2,1)S(1)}, bf16[256,2048]{1,0:T(8,128)(2,1)}, u32[]{:S(2)}) copy-start(bf16[256,2048]{1,0:T(8,128)(2,1)} %w_up.1) | copy-start | bytes 3145732
  21.3 29.9 %copy-start.10 = (f32[256]{0:T(256)S(1)}, f32[256]{0:T(256)}, u32[]{:S(2)}) copy-start(f32[256]{0:T(256)} %param.25) | copy-start | bytes 3076
  21.3 51.2 %copy-start.2 = (bf16[2048,256]{1,0:T(8,128)(2,1)S(1)}, bf16[2048,256]{1,0:T(8,128)(2,1)}, u32[]{:S(2)}) copy-start(bf16[2048,256]{1,0:T(8,128)(2,1)} %w_down.1) | copy-start | bytes 3145732
  38.9 3.6 %collective-permute-start = (bf16[64,256]{1,0:T(8,128)(2,1)S(1)}, bf16[64,256]{1,0:T(8,128)(2,1)S(1)}, u32[]{:S(2)}, u32[]{:S(2)}) collective-permute-start(bf16[64,256]{1,0:T(8,128)(2,1)S(1)} %merge.1.mine), channel_id=1, source_target_pairs={{0,1},{1,0},{2,3},{3,2},{4,5},{5,4},{6,7},{7,6},{8,9},{9,8},{10,11... | collective-permute-start | bytes 98312 | tf_op jit(solution)/shard_map/ppermute | solution.py:279
  72.9 5.3 %collective-permute-start.1 = (bf16[64,256]{1,0:T(8,128)(2,1)S(1)}, bf16[64,256]{1,0:T(8,128)(2,1)S(1)}, u32[]{:S(2)}, u32[]{:S(2)}) collective-permute-start(bf16[64,256]{1,0:T(8,128)(2,1)S(1)} %down.1.mine), channel_id=1, source_target_pairs={{0,1},{1,0},{2,3},{3,2},{4,5},{5,4},{6,7},{7,6},{8,9},{9,8},{10,11... | collective-permute-start | bytes 98312 | tf_op jit(solution)/shard_map/ppermute | solution.py:279

commit v7 on v6

--- a/solution.py
+++ b/solution.py
@@ -73,10 +73,17 @@
     squares_high = high(squares)
     row_high = column_to_row(squares_high, 128, 64)
     row_low = column_to_row(squares - squares_high, 128, 64)
-    line = iota((64, 128), 0) % 8
+    line = iota((64, 128), 0) % 4
     forget = forget + jnp.where(line == 0, row_high, jnp.where(line == 1, row_low, 0.0))
-    extra_out[:, 0:128] = key_value.astype(BF)
-    extra_out[:, 128:256] = forget.astype(BF)
+    upper = iota((8, 128), 0) < 4
+    for p in range(16):
+        rows = slice(8 * (p // 2), 8 * (p // 2) + 8)
+        first, second = key_value[rows], forget[rows]
+        if p % 2 == 0:
+            second = pltpu.roll(second, 4, 0)
+        else:
+            first = pltpu.roll(first, 4, 0)
+        extra_out[8 * p : 8 * p + 8, :] = jnp.where(upper, first, second).astype(BF)
 
 
 def head_kernel(out):
@@ -85,21 +92,21 @@
 
 def spread_kernel(query, extra, out):
     for p in range(16):
-        out[p, 0:64, :] = query[...]
-        out[p, 64:72, :] = extra[8 * (p // 2) : 8 * (p // 2) + 8, :]
+        out[p, 0:64, :] = query[:, 0:128]
+        out[p, 64:128, :] = query[:, 128:256]
+        out[p, 128:136, :] = extra[8 * p : 8 * p + 8, :]
 
 
 def attend_kernel(
     parts, query_gain, keys, values, decay, out,
     scales, query_rows, left, peaks, masses,
 ):
-    extra = [parts[i, 64:72, :].astype(F32) for i in range(16)]
-    raw = [parts[i, 0:64, :].astype(F32) for i in range(16)]
-    while len(raw) > 1:
-        raw = [a + b for a, b in zip(raw[::2], raw[1::2])]
-        extra = [a + b for a, b in zip(extra[::2], extra[1::2])]
-    raw, extra = raw[0], extra[0]
-    squares = row_to_column(extra[0:1, 128:256] + extra[1:2, 128:256], 64, 64)
+    total = [parts[i].astype(F32) for i in range(16)]
+    while len(total) > 1:
+        total = [a + b for a, b in zip(total[::2], total[1::2])]
+    raw = jnp.concatenate([total[0][0:64], total[0][64:128]], axis=1)
+    extra = total[0][128:136]
+    squares = row_to_column(extra[4:5] + extra[5:6], 64, 64)
     scale = lax.rsqrt(squares / D + EPS)
     scales[...] = jnp.broadcast_to(scale, (64, 128))
     head_of = iota((64, 256), 1) // HEAD_DIM
@@ -124,25 +131,25 @@
     left[...] = jnp.where(block, wide * (HEAD_DIM ** (-0.5)), 0.0).astype(BF)
 
     me = lax.axis_index("kv")
-    tile = me // 2
-    own_scale = scales[pl.ds(pl.multiple_of(8 * tile, 8), 8), :]
-    key_value = (own_scale * extra[:, 0:128]).astype(BF)
-    forget = extra[:, 128:256]
+    own_scale = scales[pl.ds(pl.multiple_of(8 * (me // 2), 8), 8), :]
+    own_scale = jnp.where(me % 2 == 0, own_scale, pltpu.roll(own_scale, 4, 0))
+    key_value = (own_scale * extra).astype(BF)
+    forget = pltpu.roll(extra, 4, 0)
     forget = own_scale * (forget + pltpu.roll(forget, 124, 1))
     log_forget = -(jnp.maximum(-forget, 0.0) + jnp.log1p(jnp.exp(-jnp.abs(forget))))
-    log_forget = jnp.where(iota((8, 128), 1) < 4, log_forget, 0.0)
-    repeat8 = iota((128, 8), 0) // 4 % 8 == iota((128, 8), 1)
-    key_value = dot(repeat8.astype(BF), key_value)
+    log_forget = jnp.where((iota((8, 128), 1) < 4) & (iota((8, 128), 0) < 4), log_forget, 0.0)
+    repeat4 = iota((128, 8), 0) // 4 % 4 == iota((128, 8), 1)
+    key_value = dot(repeat4.astype(BF), key_value)
     log_forget = jnp.dot(
-        repeat8[0:32].astype(F32), log_forget, preferred_element_type=F32, precision=lax.Precision.HIGHEST
+        repeat4[0:16].astype(F32), log_forget, preferred_element_type=F32, precision=lax.Precision.HIGHEST
     )
-    mine = iota((32, 128), 1) == iota((32, 128), 0) % 4
+    mine = iota((16, 128), 1) == iota((16, 128), 0) % 4
     log_forget = jnp.sum(jnp.where(mine, log_forget, 0.0), axis=1, keepdims=True)
-    at = pl.ds(pl.multiple_of(32 * tile, 32), 32)
-    lower = iota((32, 128), 1) < 64
-    own = jnp.sum(jnp.where(lower, query_rows[at, :] * key_value[0:32], 0.0), axis=1, keepdims=True)
+    at = pl.ds(pl.multiple_of(16 * me, 16), 16)
+    lower = iota((16, 128), 1) < 64
+    own = jnp.sum(jnp.where(lower, query_rows[at, :] * key_value[0:16], 0.0), axis=1, keepdims=True)
     own = own * (HEAD_DIM ** (-0.5)) - log_forget
-    own = jnp.concatenate([own] * 4, axis=0)
+    own = jnp.concatenate([own] * 8, axis=0)
     place = iota((128, 128), 0) == iota((128, 128), 1)
     own = jnp.sum(jnp.where(place, own, 0.0), axis=0, keepdims=True)
     pick = (iota((64, 128), 1) == iota((64, 128), 0) + 64).astype(BF)
@@ -174,14 +181,13 @@
     sums = [jnp.concatenate(folds[8 * j : 8 * j + 8], axis=1) for j in range(2)]
 
     line = iota((8, 128), 0)
-    slot = iota((1, 128), 1) // 32
+    slot = iota((1, 128), 1) // 16
     packed = jnp.zeros((8, 128), F32)
     for j in range(2):
         rows = slice(128 * j, 128 * j + 128)
         peak = jnp.sum(jnp.where(place, peaks[rows, :], 0.0), axis=0, keepdims=True)
         mass = jnp.sum(jnp.where(place, masses[rows, :], 0.0), axis=0, keepdims=True)
-        here = (slot + 4 * j == tile) & (me % 2 == 0)
-        joined = jnp.where(here, own, peak - 1e30)
+        joined = jnp.where(slot + 8 * j == me, own, peak - 1e30)
         top = jnp.maximum(peak, joined)
         keep = jnp.exp(peak - top)
         weight = jnp.exp(joined - top)
@@ -314,8 +320,8 @@
     shape = jax.ShapeDtypeStruct
     head = call(head_kernel, shape((8, 128), F32), "head", cost=3 * 10**9)()
     operands = (tokens, mix_gain.reshape(1, -1), w_query, w_key.T, w_value.T, w_forget.T)
-    query, extra = call(project_kernel, (shape((64, 256), BF), shape((64, 256), BF)), "project")(head, *operands)
-    message = call(spread_kernel, shape((16, 72, 256), BF), "spread", cost=10**10)(query, extra)
+    query, extra = call(project_kernel, (shape((64, 256), BF), shape((128, 128), BF)), "project")(head, *operands)
+    message = call(spread_kernel, shape((16, 136, 128), BF), "spread", cost=10**10)(query, extra)
     message = exchange(message, "kv")
     part = attend(message, query_gain, key_cache, value_cache, decay_cache)
     partial = call(merge_kernel, shape((64, 256), BF), "merge")(sent(part, "kv"), w_out)

time: 86.5 us -> 86.2 us (level)
  no operation moved by 1% of the time
where the time goes in v7:
time: 86.2 us; the launch traced here: 85.8 us
  blocking collectives  69.8 us (81%)
  starting transfers between devices  7.07 us (8%)
  Pallas kernels  5.91 us (7%)
  waiting for transfers between devices  1.72 us (2%)
  local copies, waits for them, and re-layouts  1.06 us (1%)
    all_to_all x6, blocking collectives, exchange(): return lax.all_to_all(array, axis, split_axis=0, concat_axis=0, tiled=True)  69.8 us
    ppermute x2, starting transfers between devices, pair_sum(): partner = lax.ppermute(partial, 'core', [(0, 1), (1, 0)])  7.07 us
    pallas_call x11, Pallas kernels, run(): pl.pallas_call(kernel, out_shape=outs, in_specs=in_specs or [VM] * len(ar...  5.91 us
  transfers between devices with their start and end apart: 2, of which 2 were waited for; matrix products, arithmetic and copies ran while one was open for 0% of the time, Pallas kernels for 0%

profile of v7, /device:TPU:1, one launch (start us, length us, event | category | flops | bytes accessed | tf_op | source)
XLA Modules:
  0.0 85.8 jit_solution(14349537150615511128)
XLA Ops:
  0.1 0.7 copy-done.5
  0.8 0.0 copy-done.7
  0.8 0.0 copy-done.6
  0.8 0.2 copy-done.3
  1.0 0.2 project.1
  1.2 0.0 slice-start.3
  1.2 0.1 spread.1
  1.3 19.8 %all_to_all.30.parts = bf16[16,136,128]{2,1,0:T(8,128)(2,1)S(1)} all-to-all(bf16[16,136,128]{2,1,0:T(8,128)(2,1)S(1)} %spread.1), channel_id=1, replica_groups=mesh['kv'=16,'x'=4,'core'=2] {'kv'}, dimensions={0} | all-to-all | bytes 1114112 | tf_op jit(solution)/shard_map/all_to_all | solution.py:281
  21.3 3.8 %attend.1 = bf16[136,128]{1,0:T(8,128)(2,1)S(1)} custom-call(bf16[16,136,128]{2,1,0:T(8,128)(2,1)S(1)} %all_to_all.30.parts, f32[1,64]{1,0:T(1,128)S(1)} %bitcast.19, bf16[4096,1024]{1,0:T(8,128)(2,1)S(1)} %bitcast.10, bf16[4096,1024]{1,0:T(8,128)(2,1)S(1)} %bitcast.13, f32[64,4,1024]{2,1,0:T(4,128)S(1)} %copy-done), custom_call_target="tpu_custom_call" | custom-call | tf_op jit(solution)/shard_map/attend/pallas_call | solution.py:49
  25.1 0.1 broadcast_in_dim.3
  25.1 13.2 %all_to_all.31.parts = bf16[16,136,128]{2,1,0:T(8,128)(2,1)S(1)} all-to-all(bf16[16,136,128]{2,1,0:T(8,128)(2,1)S(1)} %broadcast_in_dim.3), channel_id=1, replica_groups=mesh['kv'=16,'x'=4,'core'=2] {'kv'}, dimensions={0} | all-to-all | bytes 1114112 | tf_op jit(solution)/shard_map/all_to_all | solution.py:281
  38.3 0.5 merge.1.mine
  38.8 2.7 %collective-permute-start = (bf16[64,256]{1,0:T(8,128)(2,1)S(1)}, bf16[64,256]{1,0:T(8,128)(2,1)S(1)}, u32[]{:S(2)}, u32[]{:S(2)}) collective-permute-start(bf16[64,256]{1,0:T(8,128)(2,1)S(1)} %merge.1.mine), channel_id=1, source_target_pairs={{0,1},{1,0},{2,3},{3,2},{4,5},{5,4},{6,7},{7,6},{8,9},{9,8},{10,11... | collective-permute-start | bytes 98312 | tf_op jit(solution)/shard_map/ppermute | solution.py:285
  41.5 0.9 %collective-permute-done.partner = bf16[64,256]{1,0:T(8,128)(2,1)S(1)} collective-permute-done((bf16[64,256]{1,0:T(8,128)(2,1)S(1)}, bf16[64,256]{1,0:T(8,128)(2,1)S(1)}, u32[]{:S(2)}, u32[]{:S(2)}) %collective-permute-start) | collective-permute-done | bytes 32800 | tf_op jit(solution)/shard_map/ppermute | solution.py:285
  42.3 8.6 %all_to_all.32.parts = bf16[4,64,256]{2,1,0:T(8,128)(2,1)S(1)} all-to-all(bf16[4,64,256]{2,1,0:T(8,128)(2,1)S(1)} %pair.2), channel_id=1, replica_groups=mesh['kv'=16,'x'=4,'core'=2] {'x'}, dimensions={0} | all-to-all | bytes 262144 | tf_op jit(solution)/shard_map/all_to_all | solution.py:281
  51.0 0.3 up.1
  51.3 10.5 %all_to_all.33.parts = bf16[16,72,128]{2,1,0:T(8,128)(2,1)S(1)} all-to-all(bf16[16,72,128]{2,1,0:T(8,128)(2,1)S(1)} %get-tuple-element.11), channel_id=1, replica_groups=mesh['kv'=16,'x'=4,'core'=2] {'kv'}, dimensions={0} | all-to-all | bytes 589824 | tf_op jit(solution)/shard_map/all_to_all | solution.py:281
  61.8 0.1 hidden.1
  61.9 10.4 %all_to_all.34.parts = bf16[16,64,128]{2,1,0:T(8,128)(2,1)S(1)} all-to-all(bf16[16,64,128]{2,1,0:T(8,128)(2,1)S(1)} %hidden.1), channel_id=1, replica_groups=mesh['kv'=16,'x'=4,'core'=2] {'kv'}, dimensions={0} | all-to-all | bytes 524288 | tf_op jit(solution)/shard_map/all_to_all | solution.py:281
  72.4 0.3 down.1.mine
  72.7 4.4 %collective-permute-start.1 = (bf16[64,256]{1,0:T(8,128)(2,1)S(1)}, bf16[64,256]{1,0:T(8,128)(2,1)S(1)}, u32[]{:S(2)}, u32[]{:S(2)}) collective-permute-start(bf16[64,256]{1,0:T(8,128)(2,1)S(1)} %down.1.mine), channel_id=1, source_target_pairs={{0,1},{1,0},{2,3},{3,2},{4,5},{5,4},{6,7},{7,6},{8,9},{9,8},{10,11... | collective-permute-start | bytes 98312 | tf_op jit(solution)/shard_map/ppermute | solution.py:285
  77.1 0.9 %collective-permute-done.1.partner = bf16[64,256]{1,0:T(8,128)(2,1)S(1)} collective-permute-done((bf16[64,256]{1,0:T(8,128)(2,1)S(1)}, bf16[64,256]{1,0:T(8,128)(2,1)S(1)}, u32[]{:S(2)}, u32[]{:S(2)}) %collective-permute-start.1) | collective-permute-done | bytes 32800 | tf_op jit(solution)/shard_map/ppermute | solution.py:285
  77.9 7.2 %all_to_all.35.parts = bf16[4,64,256]{2,1,0:T(8,128)(2,1)S(1)} all-to-all(bf16[4,64,256]{2,1,0:T(8,128)(2,1)S(1)} %pair.3), channel_id=1, replica_groups=mesh['kv'=16,'x'=4,'core'=2] {'x'}, dimensions={0} | all-to-all | bytes 262144 | tf_op jit(solution)/shard_map/all_to_all | solution.py:281
  85.2 0.6 finish.1
  (32 shorter events, 0.1 us)
Async XLA Ops:
  0.0 0.8 copy-start.5
  0.0 0.8 copy-start.8
  0.0 0.8 copy-start.7
  0.0 0.8 copy-start.6
  0.0 1.0 %copy-start.3 = (bf16[256,256]{1,0:T(8,128)(2,1)S(1)}, bf16[256,256]{1,0:T(8,128)(2,1)}, u32[]{:S(2)}) copy-start(bf16[256,256]{1,0:T(8,128)(2,1)} %w_query.1) | copy-start | bytes 393220
  0.0 1.0 %copy-start.9 = (f32[256]{0:T(256)S(1)}, f32[256]{0:T(256)}, u32[]{:S(2)}) copy-start(f32[256]{0:T(256)} %param.15) | copy-start | bytes 3076
  0.0 21.1 %slice-start = ((s8[8388608]{0:T(1024)(128)(4,1)}), s8[4194304]{0:T(1024)(128)(4,1)S(1)}, s32[]{:S(2)}) async-start(s8[8388608]{0:T(1024)(128)(4,1)} %bitcast.8), calls=%async_computation.6 | async-start | bytes 8388608
  0.1 21.1 %slice-start.2 = ((s8[8388608]{0:T(1024)(128)(4,1)}), s8[4194304]{0:T(1024)(128)(4,1)S(1)}, s32[]{:S(2)}) async-start(s8[8388608]{0:T(1024)(128)(4,1)} %bitcast.11), calls=%async_computation.8 | async-start | bytes 8388608
  1.2 20.0 %slice-start.1 = ((s8[8388608]{0:T(1024)(128)(4,1)}), s8[4194304]{0:T(1024)(128)(4,1)S(1)}, s32[]{:S(2)}) async-start(s8[8388608]{0:T(1024)(128)(4,1)} %bitcast.8), calls=%async_computation.7 | async-start | bytes 8388608
  1.2 20.0 %slice-start.3 = ((s8[8388608]{0:T(1024)(128)(4,1)}), s8[4194304]{0:T(1024)(128)(4,1)S(1)}, s32[]{:S(2)}) async-start(s8[8388608]{0:T(1024)(128)(4,1)} %bitcast.11), calls=%async_computation.9 | async-start | bytes 8388608
  1.2 20.0 %copy-start = (f32[64,4,1024]{2,1,0:T(4,128)S(1)}, f32[64,4,1024]{2,1,0:T(4,128)}, u32[]{:S(2)}) copy-start(f32[64,4,1024]{2,1,0:T(4,128)} %decay.1) | copy-start | bytes 3145732
  1.2 20.0 %copy-start.11 = (f32[64]{0:T(128)S(1)}, f32[64]{0:T(128)}, u32[]{:S(2)}) copy-start(f32[64]{0:T(128)} %param.20) | copy-start | bytes 772
  21.2 17.1 %copy-start.4 = (bf16[256,256]{1,0:T(8,128)(2,1)S(1)}, bf16[256,256]{1,0:T(8,128)(2,1)}, u32[]{:S(2)}) copy-start(bf16[256,256]{1,0:T(8,128)(2,1)} %w_out.1) | copy-start | bytes 393220
  21.2 29.7 %copy-start.1 = (bf16[256,2048]{1,0:T(8,128)(2,1)S(1)}, bf16[256,2048]{1,0:T(8,128)(2,1)}, u32[]{:S(2)}) copy-start(bf16[256,2048]{1,0:T(8,128)(2,1)} %w_up.1) | copy-start | bytes 3145732
  21.2 29.7 %copy-start.10 = (f32[256]{0:T(256)S(1)}, f32[256]{0:T(256)}, u32[]{:S(2)}) copy-start(f32[256]{0:T(256)} %param.25) | copy-start | bytes 3076
  21.3 51.1 %copy-start.2 = (bf16[2048,256]{1,0:T(8,128)(2,1)S(1)}, bf16[2048,256]{1,0:T(8,128)(2,1)}, u32[]{:S(2)}) copy-start(bf16[2048,256]{1,0:T(8,128)(2,1)} %w_down.1) | copy-start | bytes 3145732
  38.8 3.5 %collective-permute-start = (bf16[64,256]{1,0:T(8,128)(2,1)S(1)}, bf16[64,256]{1,0:T(8,128)(2,1)S(1)}, u32[]{:S(2)}, u32[]{:S(2)}) collective-permute-start(bf16[64,256]{1,0:T(8,128)(2,1)S(1)} %merge.1.mine), channel_id=1, source_target_pairs={{0,1},{1,0},{2,3},{3,2},{4,5},{5,4},{6,7},{7,6},{8,9},{9,8},{10,11... | collective-permute-start | bytes 98312 | tf_op jit(solution)/shard_map/ppermute | solution.py:285
  72.7 5.3 %collective-permute-start.1 = (bf16[64,256]{1,0:T(8,128)(2,1)S(1)}, bf16[64,256]{1,0:T(8,128)(2,1)S(1)}, u32[]{:S(2)}, u32[]{:S(2)}) collective-permute-start(bf16[64,256]{1,0:T(8,128)(2,1)S(1)} %down.1.mine), channel_id=1, source_target_pairs={{0,1},{1,0},{2,3},{3,2},{4,5},{5,4},{6,7},{7,6},{8,9},{9,8},{10,11... | collective-permute-start | bytes 98312 | tf_op jit(solution)/shard_map/ppermute | solution.py:285

commit v8 on v7

--- a/solution.py
+++ b/solution.py
@@ -99,7 +99,7 @@
 
 def attend_kernel(
     parts, query_gain, keys, values, decay, out,
-    scales, query_rows, left, peaks, masses,
+    scales, query_rows, peaks, masses,
 ):
     total = [parts[i].astype(F32) for i in range(16)]
     while len(total) > 1:
@@ -113,7 +113,9 @@
     power = raw * raw
     inverse = jnp.zeros((64, 256), F32)
     for h in range(4):
-        mean = jnp.sum(jnp.where(head_of == h, power, 0.0), axis=1, keepdims=True) / HEAD_DIM
+        half = power[:, 128 * (h // 2) : 128 * (h // 2) + 128]
+        half = jnp.where(iota((64, 128), 1) // HEAD_DIM == h % 2, half, 0.0)
+        mean = jnp.sum(half, axis=1, keepdims=True) / HEAD_DIM
         inverse = jnp.where(head_of == h, scale * lax.rsqrt(scale * scale * mean + EPS), inverse)
     gain = query_gain[...]
     gain = jnp.concatenate([gain, gain, gain, gain], axis=1)
@@ -128,7 +130,7 @@
     query_rows[...] = folded
     wide = jnp.concatenate([folded] * 2, axis=1)
     block = iota((256, 256), 1) // HEAD_DIM == (iota((256, 256), 0) // 4) % 4
-    left[...] = jnp.where(block, wide * (HEAD_DIM ** (-0.5)), 0.0).astype(BF)
+    left = jnp.where(block, wide * (HEAD_DIM ** (-0.5)), 0.0).astype(BF)
 
     me = lax.axis_index("kv")
     own_scale = scales[pl.ds(pl.multiple_of(8 * (me // 2), 8), 8), :]
@@ -158,7 +160,7 @@
     lane = iota((64, 16), 1)
     folds = []
     def score(g):
-        scores = dot(left[16 * g : 16 * g + 16, :], keys[256 * g : 256 * g + 256, :])
+        scores = dot(left[16 * g : 16 * g + 16], keys[256 * g : 256 * g + 256, :])
         return scores + decay[4 * g : 4 * g + 4].reshape(16, 1024)
 
     ahead = [score(g) for g in range(8)]
@@ -192,13 +194,17 @@
         keep = jnp.exp(peak - top)
         weight = jnp.exp(joined - top)
         mass = mass * keep + weight
-        out[64 * j : 64 * j + 64, :] = ((sums[j] * keep + high(weight) * value) / mass).astype(BF)
+        result = ((sums[j] * keep + high(weight) * value) / mass).astype(BF)
+        for i in range(16):
+            out[i, 64 * j : 64 * j + 64, :] = result
         level = top + jnp.log(mass)
         for k in range(3):
             piece = high(level)
             packed = jnp.where(line == 3 * j + k, piece, packed)
             level = level - piece
-    out[128:136, :] = packed.astype(BF)
+    packed = packed.astype(BF)
+    for i in range(16):
+        out[i, 128:136, :] = packed
 
 
 def merge_kernel(parts, w_out, out):
@@ -287,19 +293,14 @@
     return exchange(message, "x")
 
 
-def sent(array, axis):
-    return exchange(jnp.broadcast_to(array, (lax.axis_size(axis), *array.shape)), axis)
-
-
 def attend(message, query_gain, key_cache, value_cache, decay_cache):
     return call(
         attend_kernel,
-        jax.ShapeDtypeStruct((136, 128), BF),
+        jax.ShapeDtypeStruct((16, 136, 128), BF),
         "attend",
         scratch=[
             pltpu.VMEM((64, 128), F32),
             pltpu.VMEM((256, 128), F32),
-            pltpu.VMEM((256, 256), BF),
             pltpu.VMEM((256, 128), F32),
             pltpu.VMEM((256, 128), F32),
         ],
@@ -324,7 +325,7 @@
     message = call(spread_kernel, shape((16, 136, 128), BF), "spread", cost=10**10)(query, extra)
     message = exchange(message, "kv")
     part = attend(message, query_gain, key_cache, value_cache, decay_cache)
-    partial = call(merge_kernel, shape((64, 256), BF), "merge")(sent(part, "kv"), w_out)
+    partial = call(merge_kernel, shape((64, 256), BF), "merge")(exchange(part, "kv"), w_out)
     residual, message = call(up_kernel, (shape((64, 256), BF), shape((16, 72, 128), BF)), "up")(
         pair_sum(partial), tokens, mlp_gain.reshape(1, -1), w_up
     )

time: 86.2 us -> 86.1 us (level)
  no operation moved by 1% of the time
where the time goes in v8:
time: 86.1 us; the launch traced here: 85.7 us
  blocking collectives  69.8 us (81%)
  starting transfers between devices  7.07 us (8%)
  Pallas kernels  5.91 us (7%)
  waiting for transfers between devices  1.72 us (2%)
  local copies, waits for them, and re-layouts  0.98 us (1%)
    all_to_all x6, blocking collectives, exchange(): return lax.all_to_all(array, axis, split_axis=0, concat_axis=0, tiled=True)  69.8 us
    ppermute x2, starting transfers between devices, pair_sum(): partner = lax.ppermute(partial, 'core', [(0, 1), (1, 0)])  7.07 us
    pallas_call x11, Pallas kernels, run(): pl.pallas_call(kernel, out_shape=outs, in_specs=in_specs or [VM] * len(ar...  5.91 us
  transfers between devices with their start and end apart: 2, of which 2 were waited for; matrix products, arithmetic and copies ran while one was open for 0% of the time, Pallas kernels for 0%

profile of v8, /device:TPU:1, one launch (start us, length us, event | category | flops | bytes accessed | tf_op | source)
XLA Modules:
  0.0 85.7 jit_solution(5745165964263532407)
XLA Ops:
  0.1 0.7 copy-done.5
  0.8 0.0 copy-done.7
  0.8 0.0 copy-done.6
  0.8 0.2 copy-done.3
  1.0 0.2 project.1
  1.2 0.0 slice-start.1
  1.2 0.0 slice-start.3
  1.2 0.1 spread.1
  1.3 19.8 %all_to_all.30.parts = bf16[16,136,128]{2,1,0:T(8,128)(2,1)S(1)} all-to-all(bf16[16,136,128]{2,1,0:T(8,128)(2,1)S(1)} %spread.1), channel_id=1, replica_groups=mesh['kv'=16,'x'=4,'core'=2] {'kv'}, dimensions={0} | all-to-all | bytes 1114112 | tf_op jit(solution)/shard_map/all_to_all | solution.py:287
  21.3 3.8 %attend.1 = bf16[16,136,128]{2,1,0:T(8,128)(2,1)S(1)} custom-call(bf16[16,136,128]{2,1,0:T(8,128)(2,1)S(1)} %all_to_all.30.parts, f32[1,64]{1,0:T(1,128)S(1)} %bitcast.19, bf16[4096,1024]{1,0:T(8,128)(2,1)S(1)} %bitcast.10, bf16[4096,1024]{1,0:T(8,128)(2,1)S(1)} %bitcast.13, f32[64,4,1024]{2,1,0:T(4,128)S(1)} %copy-done), custom_call_target="tpu_custom_call" | custom-call | tf_op jit(solution)/shard_map/attend/pallas_call | solution.py:49
  25.0 13.2 %all_to_all.31.parts = bf16[16,136,128]{2,1,0:T(8,128)(2,1)S(1)} all-to-all(bf16[16,136,128]{2,1,0:T(8,128)(2,1)S(1)} %attend.1), channel_id=1, replica_groups=mesh['kv'=16,'x'=4,'core'=2] {'kv'}, dimensions={0} | all-to-all | bytes 1114112 | tf_op jit(solution)/shard_map/all_to_all | solution.py:287
  38.2 0.5 merge.1.mine
  38.7 2.7 %collective-permute-start = (bf16[64,256]{1,0:T(8,128)(2,1)S(1)}, bf16[64,256]{1,0:T(8,128)(2,1)S(1)}, u32[]{:S(2)}, u32[]{:S(2)}) collective-permute-start(bf16[64,256]{1,0:T(8,128)(2,1)S(1)} %merge.1.mine), channel_id=1, source_target_pairs={{0,1},{1,0},{2,3},{3,2},{4,5},{5,4},{6,7},{7,6},{8,9},{9,8},{10,11... | collective-permute-start | bytes 98312 | tf_op jit(solution)/shard_map/ppermute | solution.py:291
  41.4 0.9 %collective-permute-done.partner = bf16[64,256]{1,0:T(8,128)(2,1)S(1)} collective-permute-done((bf16[64,256]{1,0:T(8,128)(2,1)S(1)}, bf16[64,256]{1,0:T(8,128)(2,1)S(1)}, u32[]{:S(2)}, u32[]{:S(2)}) %collective-permute-start) | collective-permute-done | bytes 32800 | tf_op jit(solution)/shard_map/ppermute | solution.py:291
  42.2 8.6 %all_to_all.32.parts = bf16[4,64,256]{2,1,0:T(8,128)(2,1)S(1)} all-to-all(bf16[4,64,256]{2,1,0:T(8,128)(2,1)S(1)} %pair.2), channel_id=1, replica_groups=mesh['kv'=16,'x'=4,'core'=2] {'x'}, dimensions={0} | all-to-all | bytes 262144 | tf_op jit(solution)/shard_map/all_to_all | solution.py:287
  50.9 0.3 up.1
  51.2 10.5 %all_to_all.33.parts = bf16[16,72,128]{2,1,0:T(8,128)(2,1)S(1)} all-to-all(bf16[16,72,128]{2,1,0:T(8,128)(2,1)S(1)} %get-tuple-element.11), channel_id=1, replica_groups=mesh['kv'=16,'x'=4,'core'=2] {'kv'}, dimensions={0} | all-to-all | bytes 589824 | tf_op jit(solution)/shard_map/all_to_all | solution.py:287
  61.7 0.1 hidden.1
  61.8 10.4 %all_to_all.34.parts = bf16[16,64,128]{2,1,0:T(8,128)(2,1)S(1)} all-to-all(bf16[16,64,128]{2,1,0:T(8,128)(2,1)S(1)} %hidden.1), channel_id=1, replica_groups=mesh['kv'=16,'x'=4,'core'=2] {'kv'}, dimensions={0} | all-to-all | bytes 524288 | tf_op jit(solution)/shard_map/all_to_all | solution.py:287
  72.3 0.3 down.1.mine
  72.6 4.4 %collective-permute-start.1 = (bf16[64,256]{1,0:T(8,128)(2,1)S(1)}, bf16[64,256]{1,0:T(8,128)(2,1)S(1)}, u32[]{:S(2)}, u32[]{:S(2)}) collective-permute-start(bf16[64,256]{1,0:T(8,128)(2,1)S(1)} %down.1.mine), channel_id=1, source_target_pairs={{0,1},{1,0},{2,3},{3,2},{4,5},{5,4},{6,7},{7,6},{8,9},{9,8},{10,11... | collective-permute-start | bytes 98312 | tf_op jit(solution)/shard_map/ppermute | solution.py:291
  77.0 0.9 %collective-permute-done.1.partner = bf16[64,256]{1,0:T(8,128)(2,1)S(1)} collective-permute-done((bf16[64,256]{1,0:T(8,128)(2,1)S(1)}, bf16[64,256]{1,0:T(8,128)(2,1)S(1)}, u32[]{:S(2)}, u32[]{:S(2)}) %collective-permute-start.1) | collective-permute-done | bytes 32800 | tf_op jit(solution)/shard_map/ppermute | solution.py:291
  77.9 7.2 %all_to_all.35.parts = bf16[4,64,256]{2,1,0:T(8,128)(2,1)S(1)} all-to-all(bf16[4,64,256]{2,1,0:T(8,128)(2,1)S(1)} %pair.3), channel_id=1, replica_groups=mesh['kv'=16,'x'=4,'core'=2] {'x'}, dimensions={0} | all-to-all | bytes 262144 | tf_op jit(solution)/shard_map/all_to_all | solution.py:287
  85.1 0.6 finish.1
  (31 shorter events, 0.1 us)
Async XLA Ops:
  0.0 0.8 copy-start.5
  0.0 0.8 copy-start.8
  0.0 0.8 copy-start.7
  0.0 0.8 copy-start.6
  0.0 1.0 %copy-start.3 = (bf16[256,256]{1,0:T(8,128)(2,1)S(1)}, bf16[256,256]{1,0:T(8,128)(2,1)}, u32[]{:S(2)}) copy-start(bf16[256,256]{1,0:T(8,128)(2,1)} %w_query.1) | copy-start | bytes 393220
  0.0 1.0 %copy-start.9 = (f32[256]{0:T(256)S(1)}, f32[256]{0:T(256)}, u32[]{:S(2)}) copy-start(f32[256]{0:T(256)} %param.15) | copy-start | bytes 3076
  0.0 21.1 %slice-start = ((s8[8388608]{0:T(1024)(128)(4,1)}), s8[4194304]{0:T(1024)(128)(4,1)S(1)}, s32[]{:S(2)}) async-start(s8[8388608]{0:T(1024)(128)(4,1)} %bitcast.8), calls=%async_computation.6 | async-start | bytes 8388608
  0.1 21.1 %slice-start.2 = ((s8[8388608]{0:T(1024)(128)(4,1)}), s8[4194304]{0:T(1024)(128)(4,1)S(1)}, s32[]{:S(2)}) async-start(s8[8388608]{0:T(1024)(128)(4,1)} %bitcast.11), calls=%async_computation.8 | async-start | bytes 8388608
  1.2 20.0 %slice-start.1 = ((s8[8388608]{0:T(1024)(128)(4,1)}), s8[4194304]{0:T(1024)(128)(4,1)S(1)}, s32[]{:S(2)}) async-start(s8[8388608]{0:T(1024)(128)(4,1)} %bitcast.8), calls=%async_computation.7 | async-start | bytes 8388608
  1.2 20.0 %slice-start.3 = ((s8[8388608]{0:T(1024)(128)(4,1)}), s8[4194304]{0:T(1024)(128)(4,1)S(1)}, s32[]{:S(2)}) async-start(s8[8388608]{0:T(1024)(128)(4,1)} %bitcast.11), calls=%async_computation.9 | async-start | bytes 8388608
  1.2 20.0 %copy-start = (f32[64,4,1024]{2,1,0:T(4,128)S(1)}, f32[64,4,1024]{2,1,0:T(4,128)}, u32[]{:S(2)}) copy-start(f32[64,4,1024]{2,1,0:T(4,128)} %decay.1) | copy-start | bytes 3145732
  1.2 20.0 %copy-start.11 = (f32[64]{0:T(128)S(1)}, f32[64]{0:T(128)}, u32[]{:S(2)}) copy-start(f32[64]{0:T(128)} %param.20) | copy-start | bytes 772
  21.2 17.0 %copy-start.4 = (bf16[256,256]{1,0:T(8,128)(2,1)S(1)}, bf16[256,256]{1,0:T(8,128)(2,1)}, u32[]{:S(2)}) copy-start(bf16[256,256]{1,0:T(8,128)(2,1)} %w_out.1) | copy-start | bytes 393220
  21.2 29.7 %copy-start.1 = (bf16[256,2048]{1,0:T(8,128)(2,1)S(1)}, bf16[256,2048]{1,0:T(8,128)(2,1)}, u32[]{:S(2)}) copy-start(bf16[256,2048]{1,0:T(8,128)(2,1)} %w_up.1) | copy-start | bytes 3145732
  21.2 29.6 %copy-start.10 = (f32[256]{0:T(256)S(1)}, f32[256]{0:T(256)}, u32[]{:S(2)}) copy-start(f32[256]{0:T(256)} %param.25) | copy-start | bytes 3076
  21.3 51.0 %copy-start.2 = (bf16[2048,256]{1,0:T(8,128)(2,1)S(1)}, bf16[2048,256]{1,0:T(8,128)(2,1)}, u32[]{:S(2)}) copy-start(bf16[2048,256]{1,0:T(8,128)(2,1)} %w_down.1) | copy-start | bytes 3145732
  38.7 3.5 %collective-permute-start = (bf16[64,256]{1,0:T(8,128)(2,1)S(1)}, bf16[64,256]{1,0:T(8,128)(2,1)S(1)}, u32[]{:S(2)}, u32[]{:S(2)}) collective-permute-start(bf16[64,256]{1,0:T(8,128)(2,1)S(1)} %merge.1.mine), channel_id=1, source_target_pairs={{0,1},{1,0},{2,3},{3,2},{4,5},{5,4},{6,7},{7,6},{8,9},{9,8},{10,11... | collective-permute-start | bytes 98312 | tf_op jit(solution)/shard_map/ppermute | solution.py:291
  72.6 5.3 %collective-permute-start.1 = (bf16[64,256]{1,0:T(8,128)(2,1)S(1)}, bf16[64,256]{1,0:T(8,128)(2,1)S(1)}, u32[]{:S(2)}, u32[]{:S(2)}) collective-permute-start(bf16[64,256]{1,0:T(8,128)(2,1)S(1)} %down.1.mine), channel_id=1, source_target_pairs={{0,1},{1,0},{2,3},{3,2},{4,5},{5,4},{6,7},{7,6},{8,9},{9,8},{10,11... | collective-permute-start | bytes 98312 | tf_op jit(solution)/shard_map/ppermute | solution.py:291

commit v9 on v8

--- a/solution.py
+++ b/solution.py
@@ -216,10 +216,10 @@
         level = extra[:, 3 * j, :] + extra[:, 3 * j + 1, :] + extra[:, 3 * j + 2, :]
         factor = jnp.exp(level - jnp.max(level, axis=0, keepdims=True))
         factor = factor / jnp.sum(factor, axis=0, keepdims=True)
-        total = jnp.zeros((64, 128), F32)
-        for i in range(16):
-            total = total + parts[i, 64 * j : 64 * j + 64, :].astype(F32) * factor[i : i + 1, :]
-        heads.append(dot_t(order, total.astype(BF)).astype(BF))
+        total = [parts[i, 64 * j : 64 * j + 64, :].astype(F32) * factor[i : i + 1, :] for i in range(16)]
+        while len(total) > 1:
+            total = [a + b for a, b in zip(total[::2], total[1::2])]
+        heads.append(dot_t(order, total[0].astype(BF)).astype(BF))
     partial = jnp.zeros((64, 256), F32)
     for h in range(4):
         attended = jnp.concatenate([heads[0][32 * h : 32 * h + 32], heads[1][32 * h : 32 * h + 32]], axis=0)
@@ -255,11 +255,10 @@
 
 
 def hidden_kernel(parts, out):
-    up = parts[0, 0:64, :].astype(F32)
-    extra = parts[0, 64:72, :].astype(F32)
-    for i in range(1, 16):
-        up = up + parts[i, 0:64, :].astype(F32)
-        extra = extra + parts[i, 64:72, :].astype(F32)
+    total = [parts[i].astype(F32) for i in range(16)]
+    while len(total) > 1:
+        total = [a + b for a, b in zip(total[::2], total[1::2])]
+    up, extra = total[0][0:64], total[0][64:72]
     squares = row_to_column(extra[0:1] + extra[1:2], 64, 0)
     up = lax.rsqrt(squares / D + EPS) * up
     up = jnp.maximum(up, 0.0)

time: 86.1 us -> 86.1 us (level)
  no operation moved by 1% of the time
where the time goes in v9:
time: 86.1 us; the launch traced here: 85.7 us
  blocking collectives  69.8 us (81%)
  starting transfers between devices  7.07 us (8%)
  Pallas kernels  5.89 us (7%)
  waiting for transfers between devices  1.72 us (2%)
  local copies, waits for them, and re-layouts  0.98 us (1%)
    all_to_all x6, blocking collectives, exchange(): return lax.all_to_all(array, axis, split_axis=0, concat_axis=0, tiled=True)  69.8 us
    ppermute x2, starting transfers between devices, pair_sum(): partner = lax.ppermute(partial, 'core', [(0, 1), (1, 0)])  7.07 us
    pallas_call x11, Pallas kernels, run(): pl.pallas_call(kernel, out_shape=outs, in_specs=in_specs or [VM] * len(ar...  5.89 us
  transfers between devices with their start and end apart: 2, of which 2 were waited for; matrix products, arithmetic and copies ran while one was open for 0% of the time, Pallas kernels for 0%

profile of v9, /device:TPU:1, one launch (start us, length us, event | category | flops | bytes accessed | tf_op | source)
XLA Modules:
  0.0 85.7 jit_solution(11896201064230293517)
XLA Ops:
  0.1 0.7 copy-done.5
  0.8 0.0 copy-done.7
  0.8 0.0 copy-done.6
  0.8 0.2 copy-done.3
  1.0 0.2 project.1
  1.2 0.0 slice-start.1
  1.2 0.0 slice-start.3
  1.2 0.1 spread.1
  1.3 19.8 %all_to_all.30.parts = bf16[16,136,128]{2,1,0:T(8,128)(2,1)S(1)} all-to-all(bf16[16,136,128]{2,1,0:T(8,128)(2,1)S(1)} %spread.1), channel_id=1, replica_groups=mesh['kv'=16,'x'=4,'core'=2] {'kv'}, dimensions={0} | all-to-all | bytes 1114112 | tf_op jit(solution)/shard_map/all_to_all | solution.py:286
  21.3 3.8 %attend.1 = bf16[16,136,128]{2,1,0:T(8,128)(2,1)S(1)} custom-call(bf16[16,136,128]{2,1,0:T(8,128)(2,1)S(1)} %all_to_all.30.parts, f32[1,64]{1,0:T(1,128)S(1)} %bitcast.19, bf16[4096,1024]{1,0:T(8,128)(2,1)S(1)} %bitcast.10, bf16[4096,1024]{1,0:T(8,128)(2,1)S(1)} %bitcast.13, f32[64,4,1024]{2,1,0:T(4,128)S(1)} %copy-done), custom_call_target="tpu_custom_call" | custom-call | tf_op jit(solution)/shard_map/attend/pallas_call | solution.py:49
  25.0 13.2 %all_to_all.31.parts = bf16[16,136,128]{2,1,0:T(8,128)(2,1)S(1)} all-to-all(bf16[16,136,128]{2,1,0:T(8,128)(2,1)S(1)} %attend.1), channel_id=1, replica_groups=mesh['kv'=16,'x'=4,'core'=2] {'kv'}, dimensions={0} | all-to-all | bytes 1114112 | tf_op jit(solution)/shard_map/all_to_all | solution.py:286
  38.2 0.5 merge.1.mine
  38.7 2.7 %collective-permute-start = (bf16[64,256]{1,0:T(8,128)(2,1)S(1)}, bf16[64,256]{1,0:T(8,128)(2,1)S(1)}, u32[]{:S(2)}, u32[]{:S(2)}) collective-permute-start(bf16[64,256]{1,0:T(8,128)(2,1)S(1)} %merge.1.mine), channel_id=1, source_target_pairs={{0,1},{1,0},{2,3},{3,2},{4,5},{5,4},{6,7},{7,6},{8,9},{9,8},{10,11... | collective-permute-start | bytes 98312 | tf_op jit(solution)/shard_map/ppermute | solution.py:290
  41.4 0.9 %collective-permute-done.partner = bf16[64,256]{1,0:T(8,128)(2,1)S(1)} collective-permute-done((bf16[64,256]{1,0:T(8,128)(2,1)S(1)}, bf16[64,256]{1,0:T(8,128)(2,1)S(1)}, u32[]{:S(2)}, u32[]{:S(2)}) %collective-permute-start) | collective-permute-done | bytes 32800 | tf_op jit(solution)/shard_map/ppermute | solution.py:290
  42.2 8.6 %all_to_all.32.parts = bf16[4,64,256]{2,1,0:T(8,128)(2,1)S(1)} all-to-all(bf16[4,64,256]{2,1,0:T(8,128)(2,1)S(1)} %pair.2), channel_id=1, replica_groups=mesh['kv'=16,'x'=4,'core'=2] {'x'}, dimensions={0} | all-to-all | bytes 262144 | tf_op jit(solution)/shard_map/all_to_all | solution.py:286
  50.9 0.3 up.1
  51.2 10.5 %all_to_all.33.parts = bf16[16,72,128]{2,1,0:T(8,128)(2,1)S(1)} all-to-all(bf16[16,72,128]{2,1,0:T(8,128)(2,1)S(1)} %get-tuple-element.11), channel_id=1, replica_groups=mesh['kv'=16,'x'=4,'core'=2] {'kv'}, dimensions={0} | all-to-all | bytes 589824 | tf_op jit(solution)/shard_map/all_to_all | solution.py:286
  61.7 0.1 hidden.1
  61.8 10.4 %all_to_all.34.parts = bf16[16,64,128]{2,1,0:T(8,128)(2,1)S(1)} all-to-all(bf16[16,64,128]{2,1,0:T(8,128)(2,1)S(1)} %hidden.1), channel_id=1, replica_groups=mesh['kv'=16,'x'=4,'core'=2] {'kv'}, dimensions={0} | all-to-all | bytes 524288 | tf_op jit(solution)/shard_map/all_to_all | solution.py:286
  72.2 0.3 down.1.mine
  72.6 4.4 %collective-permute-start.1 = (bf16[64,256]{1,0:T(8,128)(2,1)S(1)}, bf16[64,256]{1,0:T(8,128)(2,1)S(1)}, u32[]{:S(2)}, u32[]{:S(2)}) collective-permute-start(bf16[64,256]{1,0:T(8,128)(2,1)S(1)} %down.1.mine), channel_id=1, source_target_pairs={{0,1},{1,0},{2,3},{3,2},{4,5},{5,4},{6,7},{7,6},{8,9},{9,8},{10,11... | collective-permute-start | bytes 98312 | tf_op jit(solution)/shard_map/ppermute | solution.py:290
  77.0 0.9 %collective-permute-done.1.partner = bf16[64,256]{1,0:T(8,128)(2,1)S(1)} collective-permute-done((bf16[64,256]{1,0:T(8,128)(2,1)S(1)}, bf16[64,256]{1,0:T(8,128)(2,1)S(1)}, u32[]{:S(2)}, u32[]{:S(2)}) %collective-permute-start.1) | collective-permute-done | bytes 32800 | tf_op jit(solution)/shard_map/ppermute | solution.py:290
  77.8 7.2 %all_to_all.35.parts = bf16[4,64,256]{2,1,0:T(8,128)(2,1)S(1)} all-to-all(bf16[4,64,256]{2,1,0:T(8,128)(2,1)S(1)} %pair.3), channel_id=1, replica_groups=mesh['kv'=16,'x'=4,'core'=2] {'x'}, dimensions={0} | all-to-all | bytes 262144 | tf_op jit(solution)/shard_map/all_to_all | solution.py:286
  85.1 0.6 finish.1
  (31 shorter events, 0.1 us)
Async XLA Ops:
  0.0 0.8 copy-start.5
  0.0 0.8 copy-start.8
  0.0 0.8 copy-start.7
  0.0 0.8 copy-start.6
  0.0 1.0 %copy-start.3 = (bf16[256,256]{1,0:T(8,128)(2,1)S(1)}, bf16[256,256]{1,0:T(8,128)(2,1)}, u32[]{:S(2)}) copy-start(bf16[256,256]{1,0:T(8,128)(2,1)} %w_query.1) | copy-start | bytes 393220
  0.0 1.0 %copy-start.9 = (f32[256]{0:T(256)S(1)}, f32[256]{0:T(256)}, u32[]{:S(2)}) copy-start(f32[256]{0:T(256)} %param.15) | copy-start | bytes 3076
  0.0 21.1 %slice-start = ((s8[8388608]{0:T(1024)(128)(4,1)}), s8[4194304]{0:T(1024)(128)(4,1)S(1)}, s32[]{:S(2)}) async-start(s8[8388608]{0:T(1024)(128)(4,1)} %bitcast.8), calls=%async_computation.6 | async-start | bytes 8388608
  0.1 21.1 %slice-start.2 = ((s8[8388608]{0:T(1024)(128)(4,1)}), s8[4194304]{0:T(1024)(128)(4,1)S(1)}, s32[]{:S(2)}) async-start(s8[8388608]{0:T(1024)(128)(4,1)} %bitcast.11), calls=%async_computation.8 | async-start | bytes 8388608
  1.2 20.0 %slice-start.1 = ((s8[8388608]{0:T(1024)(128)(4,1)}), s8[4194304]{0:T(1024)(128)(4,1)S(1)}, s32[]{:S(2)}) async-start(s8[8388608]{0:T(1024)(128)(4,1)} %bitcast.8), calls=%async_computation.7 | async-start | bytes 8388608
  1.2 20.0 %slice-start.3 = ((s8[8388608]{0:T(1024)(128)(4,1)}), s8[4194304]{0:T(1024)(128)(4,1)S(1)}, s32[]{:S(2)}) async-start(s8[8388608]{0:T(1024)(128)(4,1)} %bitcast.11), calls=%async_computation.9 | async-start | bytes 8388608
  1.2 20.0 %copy-start = (f32[64,4,1024]{2,1,0:T(4,128)S(1)}, f32[64,4,1024]{2,1,0:T(4,128)}, u32[]{:S(2)}) copy-start(f32[64,4,1024]{2,1,0:T(4,128)} %decay.1) | copy-start | bytes 3145732
  1.2 20.0 %copy-start.11 = (f32[64]{0:T(128)S(1)}, f32[64]{0:T(128)}, u32[]{:S(2)}) copy-start(f32[64]{0:T(128)} %param.20) | copy-start | bytes 772
  21.2 17.0 %copy-start.4 = (bf16[256,256]{1,0:T(8,128)(2,1)S(1)}, bf16[256,256]{1,0:T(8,128)(2,1)}, u32[]{:S(2)}) copy-start(bf16[256,256]{1,0:T(8,128)(2,1)} %w_out.1) | copy-start | bytes 393220
  21.2 29.6 %copy-start.1 = (bf16[256,2048]{1,0:T(8,128)(2,1)S(1)}, bf16[256,2048]{1,0:T(8,128)(2,1)}, u32[]{:S(2)}) copy-start(bf16[256,2048]{1,0:T(8,128)(2,1)} %w_up.1) | copy-start | bytes 3145732
  21.2 29.6 %copy-start.10 = (f32[256]{0:T(256)S(1)}, f32[256]{0:T(256)}, u32[]{:S(2)}) copy-start(f32[256]{0:T(256)} %param.25) | copy-start | bytes 3076
  21.3 51.0 %copy-start.2 = (bf16[2048,256]{1,0:T(8,128)(2,1)S(1)}, bf16[2048,256]{1,0:T(8,128)(2,1)}, u32[]{:S(2)}) copy-start(bf16[2048,256]{1,0:T(8,128)(2,1)} %w_down.1) | copy-start | bytes 3145732
  38.7 3.5 %collective-permute-start = (bf16[64,256]{1,0:T(8,128)(2,1)S(1)}, bf16[64,256]{1,0:T(8,128)(2,1)S(1)}, u32[]{:S(2)}, u32[]{:S(2)}) collective-permute-start(bf16[64,256]{1,0:T(8,128)(2,1)S(1)} %merge.1.mine), channel_id=1, source_target_pairs={{0,1},{1,0},{2,3},{3,2},{4,5},{5,4},{6,7},{7,6},{8,9},{9,8},{10,11... | collective-permute-start | bytes 98312 | tf_op jit(solution)/shard_map/ppermute | solution.py:290
  72.6 5.3 %collective-permute-start.1 = (bf16[64,256]{1,0:T(8,128)(2,1)S(1)}, bf16[64,256]{1,0:T(8,128)(2,1)S(1)}, u32[]{:S(2)}, u32[]{:S(2)}) collective-permute-start(bf16[64,256]{1,0:T(8,128)(2,1)S(1)} %down.1.mine), channel_id=1, source_target_pairs={{0,1},{1,0},{2,3},{3,2},{4,5},{5,4},{6,7},{7,6},{8,9},{9,8},{10,11... | collective-permute-start | bytes 98312 | tf_op jit(solution)/shard_map/ppermute | solution.py:290
